TPU v7x, 32 devices: a whole 2x2x4 slice. The times are simulated.
32 devices in a mesh: ep: 8 (over z, y), tp: 4 (over x, core).
Axes of the slice: x: 2, y: 2, z: 4, core: 2. Of those that a mesh axis runs over, the one named last changes fastest.
Arguments:
- query_rows: bfloat16 [1024, 1024], P('ep', 'tp'), may hold values from -10 to 10
- key_rows: bfloat16 [1024, 1024], P('ep', 'tp'), may hold values from -10 to 10
- value_rows: bfloat16 [1024, 1024], P('ep', 'tp'), may hold values from -6 to 6
- key_bias: bfloat16 [1024, 16], P('ep', 'tp'), may hold values from -24 to 4
- mixer_weight: bfloat16 [1024, 2048], P('tp'), may hold values from -0.1875 to 0.1875
- mixer_gain: float32 [2048], replicated, may hold values from 0.1 to 1.9
- routed_input: bfloat16 [3072, 2048], P(('ep', 'tp')), may hold values from -6 to 6
- entry_gain: float32 [2048], replicated, may hold values from 0.1 to 1.9
- expert_index: int32 [3072, 2], P(('ep', 'tp')), may hold values from 0 to 15, all different within a row; in each aligned block of 96 rows (0 to 95, 96 to 191, ...) at most 18 rows name the same one
- route_weights: float32 [3072, 2], P(('ep', 'tp')), may hold values from 0.1 to 1
- expert_gate: bfloat16 [16, 2048, 1024], P('ep', None, 'tp'), may hold values from -0.125 to 0.125
- expert_up: bfloat16 [16, 2048, 1024], P('ep', None, 'tp'), may hold values from -0.125 to 0.125
- expert_down: bfloat16 [16, 1024, 2048], P('ep', 'tp'), may hold values from -0.1875 to 0.1875
- shared_gate: bfloat16 [2048, 1024], P(None, 'tp'), may hold values from -0.125 to 0.125
- shared_up: bfloat16 [2048, 1024], P(None, 'tp'), may hold values from -0.125 to 0.125
- shared_down: bfloat16 [1024, 2048], P('tp'), may hold values from -0.1875 to 0.1875
- exit_gain: float32 [2048], replicated, may hold values from 0.1 to 1.9
Outputs:
- mixer_out: bfloat16 [1024, 2048], P(('ep', 'tp'))
- expert_out: bfloat16 [3072, 2048], P(('ep', 'tp'))
Inputs may be any that keep to these rules, and one draw needn't show every extreme that they name: `expert_index`: in each aligned block of 96 rows (the rows of one device) no expert is named by more than 18 rows, a bound that some block reaches; each row names 2 different experts.
All inputs are finite; a program needn't handle non-finite values.
Results may differ from a plain program's by a relative error of at most 0.012.
Values may be sent and summed in bfloat16 or wider, within the bound.
A program may use at most 128 MiB of HBM per device.

v0:
```python
import functools

import jax
import jax.numpy as jnp
from jax import lax
from jax.experimental import pallas as pl
from jax.experimental.pallas import tpu as pltpu
from jax.sharding import PartitionSpec as P

MESH = pl.DeviceIdType.MESH


def peer_places(ep_size, tp_size):
    own_ep = lax.axis_index("ep")
    own_tp = lax.axis_index("tp")
    partner = own_tp + 1 - 2 * lax.rem(own_tp, 2)
    across = lax.rem(own_tp + tp_size // 2, tp_size)
    return own_ep, own_tp, partner, across


def greet(ep_size, own_ep, own_tp, partner, across):
    barrier = pltpu.get_barrier_semaphore()

    def signal_one(step, unused):
        place = lax.rem(own_ep + step, ep_size)
        pl.semaphore_signal(barrier, inc=1, device_id=(place, own_tp), device_id_type=MESH)
        return unused

    lax.fori_loop(1, ep_size, signal_one, 0)
    for place in (partner, across):
        pl.semaphore_signal(barrier, inc=1, device_id=(own_ep, place), device_id_type=MESH)
    pl.semaphore_wait(barrier, ep_size + 1)


def send_of(source, target, send_sem, recv_sem, place):
    return pltpu.make_async_remote_copy(
        src_ref=source,
        dst_ref=target,
        send_sem=send_sem,
        recv_sem=recv_sem,
        device_id=place,
        device_id_type=MESH,
    )


def front_kernel(
    ep_size,
    tp_size,
    head_size,
    query_ref,
    kv_ref,
    normed_ref,
    outgoing_ref,
    attended_ref,
    own_all,
    arrived,
    kv_all,
    query_heads,
    carried,
    output,
    ep_send,
    ep_recv,
    kv_send,
    kv_recv,
    pair_send,
    pair_recv,
    partner_send,
    partner_recv,
    across_send,
    across_recv,
    relay_send,
    relay_recv,
    local_sem,
):
    own_ep, own_tp, partner, across = peer_places(ep_size, tp_size)
    greet(ep_size, own_ep, own_tp, partner, across)
    to_partner = (own_ep, partner)
    to_across = (own_ep, across)

    def dispatch(step):
        target = lax.rem(own_ep + step, ep_size)
        return send_of(
            outgoing_ref.at[target],
            arrived.at[own_tp, own_ep],
            ep_send.at[step],
            ep_recv.at[step],
            (target, own_tp),
        )

    def landed(step):
        source = lax.rem(own_ep - step + ep_size, ep_size)
        block = arrived.at[own_tp, source]
        return send_of(block, block, ep_send.at[step], ep_recv.at[step], (own_ep, own_tp))

    shard_rows, width = query_ref.shape
    head_count = width // head_size
    lines = ep_size // 2
    parity = lax.rem(own_ep, 2)
    own_line = own_ep // 2
    pair_ep = own_ep + 1 - 2 * parity

    def spread_kv(step):
        target = 2 * lax.rem(own_line + step, lines) + parity
        return send_of(
            kv_ref, kv_all.at[own_ep], kv_send.at[step], kv_recv.at[step], (target, own_tp)
        )

    def line_kv(step, side):
        return kv_all.at[2 * lax.rem(own_line - step + lines, lines) + side]

    def landed_kv(step):
        block = line_kv(step, parity)
        return send_of(block, block, kv_send.at[step], kv_recv.at[step], (own_ep, own_tp))

    def pair_kv(source, target, step):
        return send_of(
            source, target, pair_send.at[step], pair_recv.at[step], (pair_ep, own_tp)
        )

    def attend_block(keys_values, own):
        keys = keys_values[0:shard_rows, 0:width]
        values = keys_values[0:shard_rows, width : 2 * width]
        ahead = lax.broadcasted_iota(jnp.int32, (shard_rows, shard_rows), 0)
        behind = lax.broadcasted_iota(jnp.int32, (shard_rows, shard_rows), 1)
        later_of = jnp.where(ahead > behind, 1.0, 0.0)
        column_head = lax.broadcasted_iota(jnp.int32, (shard_rows, width), 1) // head_size
        gained = jnp.zeros((shard_rows, width), jnp.float32)
        for head in range(head_count):
            bias_row = keys_values[shard_rows + head : shard_rows + head + 1, 0:shard_rows]
            scores = lax.dot_general(
                query_heads[head],
                keys,
                (((1,), (1,)), ((), ())),
                preferred_element_type=jnp.float32,
            )
            scores = scores * head_size ** (-0.5) + bias_row.astype(jnp.float32)
            tail = jnp.log1p(jnp.exp(-jnp.abs(scores)))
            fails = -(jnp.maximum(scores, 0.0) + tail)
            if own:
                fails = jnp.where(behind < ahead, fails, 0.0)
            later = jnp.dot(
                fails,
                later_of,
                preferred_element_type=jnp.float32,
                precision=lax.Precision.HIGHEST,
            )
            weights = jnp.exp(jnp.minimum(scores, 0.0) - tail + later + carried[head])
            if own:
                weights = jnp.where(behind < ahead, weights, 0.0)
            product = jnp.dot(
                weights.astype(jnp.bfloat16), values, preferred_element_type=jnp.float32
            )
            gained = jnp.where(column_head == head, product, gained)
            carried[head] = carried[head] + jnp.sum(fails, axis=1, keepdims=True)
        output[...] = output[...] + gained

    def tp_block(holder, step):
        return arrived.at[holder, lax.rem(own_ep - step + ep_size, ep_size)]

    def tp_copy(source, target, sems, step, place):
        return send_of(source, target, sems[0].at[step], sems[1].at[step], place)

    partner_sems = (partner_send, partner_recv)
    across_sems = (across_send, across_recv)
    relay_sems = (relay_send, relay_recv)
    last = ep_size

    lax.fori_loop(1, lines, lambda step, c: (spread_kv(step).start(), c)[1], 0)
    pair_kv(kv_ref, kv_all.at[own_ep], 0).start()
    lax.fori_loop(1, ep_size, lambda step, c: (dispatch(step).start(), c)[1], 0)
    own_block = outgoing_ref.at[own_ep]
    own_slot = arrived.at[own_tp, own_ep]
    tp_copy(normed_ref, own_all.at[own_tp], across_sems, last, to_across).start()
    tp_copy(own_block, own_slot, across_sems, 0, to_across).start()
    tp_copy(normed_ref, own_all.at[own_tp], partner_sems, last, to_partner).start()
    tp_copy(own_block, own_slot, partner_sems, 0, to_partner).start()
    locals_ = [
        pltpu.make_async_copy(own_block, own_slot, local_sem.at[0]),
        pltpu.make_async_copy(normed_ref, own_all.at[own_tp], local_sem.at[1]),
    ]
    for local in locals_:
        local.start()

    output[...] = jnp.zeros_like(output)
    carried[...] = jnp.zeros_like(carried)
    head_of = lax.broadcasted_iota(jnp.int32, (shard_rows, width), 1) // head_size
    queries = query_ref[...].astype(jnp.float32)
    for head in range(head_count):
        query_heads[head] = jnp.where(head_of == head, queries, 0.0).astype(jnp.bfloat16)
    attend_block(kv_ref[...], True)

    def relay_kv(step, carry):
        landed_kv(step).wait_recv()
        block = line_kv(step, parity)
        pair_kv(block, block, step).start()
        return carry

    lax.fori_loop(1, lines, relay_kv, 0)

    def landed_pair(step, carry):
        block = line_kv(step, 1 - parity)
        pair_kv(block, block, step).wait_recv()
        return carry

    lax.fori_loop(0, lines, landed_pair, 0)

    def forward(step, carry):
        landed(step).wait_recv()
        block = tp_block(own_tp, step)
        tp_copy(block, block, across_sems, step, to_across).start()
        tp_copy(block, block, partner_sems, step, to_partner).start()

        @pl.when(step <= own_ep)
        def attend_earlier():
            attend_block(kv_all[lax.rem(own_ep - step + ep_size, ep_size)], False)

        return carry

    lax.fori_loop(1, ep_size, forward, 0)
    attended_ref[...] = output[...].astype(jnp.bfloat16)

    other_own = own_all.at[across]
    tp_copy(other_own, other_own, across_sems, last, to_across).wait_recv()
    tp_copy(other_own, other_own, relay_sems, last, to_partner).start()

    def relay(step, carry):
        block = tp_block(across, step)
        tp_copy(block, block, across_sems, step, to_across).wait_recv()
        tp_copy(block, block, relay_sems, step, to_partner).start()
        return carry

    lax.fori_loop(0, ep_size, relay, 0)

    diagonal = lax.rem(partner + tp_size // 2, tp_size)

    def finish(step, carry):
        near = tp_block(partner, step)
        far = tp_block(diagonal, step)
        tp_copy(near, near, partner_sems, step, to_partner).wait()
        tp_copy(far, far, relay_sems, step, to_partner).wait()
        tp_copy(near, near, across_sems, step, to_across).wait_send()
        return carry

    lax.fori_loop(0, ep_size, finish, 0)
    near = own_all.at[partner]
    far = own_all.at[diagonal]
    tp_copy(near, near, partner_sems, last, to_partner).wait()
    tp_copy(far, far, relay_sems, last, to_partner).wait()
    tp_copy(near, near, across_sems, last, to_across).wait_send()

    def finish_ep(step, carry):
        dispatch(step).wait_send()
        return carry

    lax.fori_loop(1, ep_size, finish_ep, 0)

    def finish_kv(step, carry):
        block = line_kv(step, parity)
        pair_kv(block, block, step).wait_send()
        return carry

    lax.fori_loop(1, lines, finish_kv, 0)
    lax.fori_loop(1, lines, lambda step, c: (spread_kv(step).wait_send(), c)[1], 0)
    pair_kv(kv_ref, kv_all.at[own_ep], 0).wait_send()
    for local in locals_:
        local.wait()


def front_exchange(ep_size, tp_size, head_size, queries, kv, normed, outgoing):
    def spread(count, value):
        return jax.ShapeDtypeStruct((count,) + value.shape, value.dtype)

    rows, width = queries.shape
    heads = width // head_size
    ep_sem = pltpu.SemaphoreType.DMA((ep_size,))
    tp_sem = pltpu.SemaphoreType.DMA((ep_size + 1,))
    vmem = pl.BlockSpec(memory_space=pltpu.VMEM)
    return pl.pallas_call(
        functools.partial(front_kernel, ep_size, tp_size, head_size),
        out_shape=(
            jax.ShapeDtypeStruct(queries.shape, jnp.bfloat16),
            spread(tp_size, normed),
            spread(tp_size, outgoing),
        ),
        in_specs=[vmem] * 4,
        out_specs=[vmem] + [pl.BlockSpec(memory_space=pl.ANY)] * 2,
        scratch_shapes=[
            pltpu.VMEM((ep_size,) + kv.shape, kv.dtype),
            pltpu.VMEM((heads, rows, width), jnp.bfloat16),
            pltpu.VMEM((heads, rows, 1), jnp.float32),
            pltpu.VMEM((rows, width), jnp.float32),
        ]
        + [ep_sem] * 6
        + [tp_sem] * 6
        + [pltpu.SemaphoreType.DMA((2,))],
        compiler_params=pltpu.CompilerParams(
            collective_id=0, has_side_effects=True, vmem_limit_bytes=48 * 1024 * 1024
        ),
        name="front_exchange",
    )(queries, kv, normed, outgoing)


def expert_kernel(capacity, block_slots, rows_ref, gate_ref, up_ref, down_ref, part_ref):
    rows = rows_ref[...]
    row_expert = (
        lax.rem(lax.broadcasted_iota(jnp.int32, (rows.shape[0], 1), 0), block_slots) // capacity
    )
    total = jnp.zeros(part_ref.shape, jnp.float32)
    for expert in range(gate_ref.shape[0]):
        gate = jnp.dot(rows, gate_ref[expert], preferred_element_type=jnp.float32)
        up = jnp.dot(rows, up_ref[expert], preferred_element_type=jnp.float32)
        hidden = gate / (1.0 + jnp.exp(-gate)) * up
        hidden = jnp.where(row_expert == expert, hidden, 0.0).astype(jnp.bfloat16)
        total = total + jnp.dot(hidden, down_ref[expert], preferred_element_type=jnp.float32)
    part_ref[...] = total.astype(jnp.bfloat16)


def expert_parts(capacity, block_slots, tile, rows, gate, up, down):
    row_total, width = rows.shape

    def whole(value):
        return pl.BlockSpec(value.shape, lambda i: (0, 0, 0))

    return pl.pallas_call(
        functools.partial(expert_kernel, capacity, block_slots),
        grid=(row_total // tile,),
        out_shape=jax.ShapeDtypeStruct((row_total, width), jnp.bfloat16),
        in_specs=[pl.BlockSpec((tile, width), lambda i: (i, 0)), whole(gate), whole(up), whole(down)],
        out_specs=pl.BlockSpec((tile, width), lambda i: (i, 0)),
        compiler_params=pltpu.CompilerParams(vmem_limit_bytes=60 * 1024 * 1024),
        name="expert_parts",
    )(rows, gate, up, down)


def back_kernel(
    ep_size,
    tp_size,
    part_ref,
    shared_ref,
    mixer_ref,
    back_ref,
    shared_out,
    mixer_out,
    near_in,
    near_shared,
    near_mixer,
    far_out,
    far_in,
    far_shared_out,
    far_shared,
    far_mixer_out,
    far_mixer,
    total,
    near_send,
    near_recv,
    far_send,
    far_recv,
    ep_send,
    ep_recv,
    local_sem,
):
    own_ep, own_tp, partner, across = peer_places(ep_size, tp_size)
    diagonal = lax.rem(partner + tp_size // 2, tp_size)
    greet(ep_size, own_ep, own_tp, partner, across)
    to_partner = (own_ep, partner)
    to_across = (own_ep, across)
    homes = (diagonal, partner)

    def place_of(step):
        return lax.rem(own_ep + 1 + step, ep_size)

    def near_copy(side, step):
        place = place_of(step)
        return send_of(
            part_ref.at[homes[side], place],
            near_in.at[side, place],
            near_send.at[side, step],
            near_recv.at[side, step],
            to_partner,
        )

    def near_small(side, source, target, slot):
        return send_of(
            source.at[homes[side]],
            target.at[side],
            near_send.at[side, slot],
            near_recv.at[side, slot],
            to_partner,
        )

    def far_copy(source, target, slot):
        return send_of(source, target, far_send.at[slot], far_recv.at[slot], to_across)

    shared_slot, mixer_slot = ep_size, ep_size + 1

    for side in range(2):
        lax.fori_loop(
            0, ep_size, lambda step, c, side=side: (near_copy(side, step).start(), c)[1], 0
        )
        near_small(side, shared_ref, near_shared, shared_slot).start()
        near_small(side, mixer_ref, near_mixer, mixer_slot).start()

    def add(left, right):
        return left.astype(jnp.float32) + right.astype(jnp.float32)

    def pass_on(step, carry):
        place = place_of(step)
        near_copy(0, step).wait_recv()
        far_out[place] = add(part_ref[across, place], near_in[0, place]).astype(jnp.bfloat16)
        far_copy(far_out.at[place], far_in.at[place], step).start()
        return carry

    lax.fori_loop(0, ep_size, pass_on, 0)
    near_small(0, shared_ref, near_shared, shared_slot).wait_recv()
    far_shared_out[...] = add(shared_ref[across], near_shared[0]).astype(jnp.bfloat16)
    far_copy(far_shared_out, far_shared, shared_slot).start()
    near_small(0, mixer_ref, near_mixer, mixer_slot).wait_recv()
    far_mixer_out[...] = add(mixer_ref[across], near_mixer[0]).astype(jnp.bfloat16)
    far_copy(far_mixer_out, far_mixer, mixer_slot).start()

    def send_back(step):
        place = place_of(step)
        return send_of(
            total.at[place],
            back_ref.at[own_ep],
            ep_send.at[step],
            ep_recv.at[step],
            (place, own_tp),
        )

    def gather_total(step):
        place = place_of(step)
        near_copy(1, step).wait_recv()
        far_copy(far_out.at[place], far_in.at[place], step).wait_recv()
        value = add(part_ref[own_tp, place], near_in[1, place]) + far_in[place].astype(jnp.float32)
        total[place] = value.astype(jnp.bfloat16)

    def return_one(step, carry):
        gather_total(step)
        send_back(step).start()
        return carry

    lax.fori_loop(0, ep_size - 1, return_one, 0)
    gather_total(ep_size - 1)
    local = pltpu.make_async_copy(total.at[own_ep], back_ref.at[own_ep], local_sem)
    local.start()

    near_small(1, shared_ref, near_shared, shared_slot).wait_recv()
    far_copy(far_shared_out, far_shared, shared_slot).wait_recv()
    shared_out[...] = add(shared_ref[own_tp], near_shared[1]) + far_shared[...].astype(jnp.float32)
    near_small(1, mixer_ref, near_mixer, mixer_slot).wait_recv()
    far_copy(far_mixer_out, far_mixer, mixer_slot).wait_recv()
    mixer_out[...] = add(mixer_ref[own_tp], near_mixer[1]) + far_mixer[...].astype(jnp.float32)

    def finish(step, carry):
        place = place_of(step)
        near_copy(0, step).wait_send()
        near_copy(1, step).wait_send()
        far_copy(far_out.at[place], far_in.at[place], step).wait_send()
        return carry

    lax.fori_loop(0, ep_size, finish, 0)
    for side in range(2):
        near_small(side, shared_ref, near_shared, shared_slot).wait_send()
        near_small(side, mixer_ref, near_mixer, mixer_slot).wait_send()
    far_copy(far_shared_out, far_shared, shared_slot).wait_send()
    far_copy(far_mixer_out, far_mixer, mixer_slot).wait_send()

    def finish_ep(step, carry):
        send_back(step).wait_send()
        source = lax.rem(own_ep - 1 - step + 2 * ep_size, ep_size)
        block = back_ref.at[source]
        send_of(
            block, block, ep_send.at[step], ep_recv.at[step], (own_ep, own_tp)
        ).wait_recv()
        return carry

    lax.fori_loop(0, ep_size - 1, finish_ep, 0)
    local.wait()


def back_exchange(ep_size, tp_size, part, shared, mixer):
    block = part.shape[2:]
    bf16 = jnp.bfloat16
    sem = pltpu.SemaphoreType.DMA
    vmem = pl.BlockSpec(memory_space=pltpu.VMEM)
    return pl.pallas_call(
        functools.partial(back_kernel, ep_size, tp_size),
        out_shape=(
            jax.ShapeDtypeStruct((ep_size,) + block, bf16),
            jax.ShapeDtypeStruct(shared.shape[1:], jnp.float32),
            jax.ShapeDtypeStruct(mixer.shape[1:], jnp.float32),
        ),
        in_specs=[vmem] * 3,
        out_specs=[pl.BlockSpec(memory_space=pl.ANY), vmem, vmem],
        scratch_shapes=[
            pltpu.VMEM((2, ep_size) + block, bf16),
            pltpu.VMEM((2,) + shared.shape[1:], bf16),
            pltpu.VMEM((2,) + mixer.shape[1:], bf16),
            pltpu.VMEM((ep_size,) + block, bf16),
            pltpu.VMEM((ep_size,) + block, bf16),
            pltpu.VMEM(shared.shape[1:], bf16),
            pltpu.VMEM(shared.shape[1:], bf16),
            pltpu.VMEM(mixer.shape[1:], bf16),
            pltpu.VMEM(mixer.shape[1:], bf16),
            pltpu.VMEM((ep_size,) + block, bf16),
            sem((2, ep_size + 2)),
            sem((2, ep_size + 2)),
            sem((ep_size + 2,)),
            sem((ep_size + 2,)),
            sem((ep_size,)),
            sem((ep_size,)),
            sem,
        ],
        compiler_params=pltpu.CompilerParams(
            collective_id=1, has_side_effects=True, vmem_limit_bytes=60 * 1024 * 1024
        ),
        name="back_exchange",
    )(part, shared, mixer)


EPS = 1e-06


def root_norm(values, gain_row):
    return values * lax.rsqrt(jnp.mean(values * values, axis=-1, keepdims=True) + EPS) * gain_row


def shared_term_of(own_all, shared_gate, shared_up, shared_down):
    gate_part = jnp.dot(own_all, shared_gate, preferred_element_type=jnp.float32)
    up_part = jnp.dot(own_all, shared_up, preferred_element_type=jnp.float32)
    hidden = (jax.nn.silu(gate_part) * up_part).astype(jnp.bfloat16)
    return jnp.dot(hidden, shared_down, preferred_element_type=jnp.float32).astype(jnp.bfloat16)


def on_device(
    query_rows,
    key_rows,
    value_rows,
    key_bias,
    mixer_weight,
    mixer_gain,
    routed_input,
    entry_gain,
    expert_index,
    route_weights,
    expert_gate,
    expert_up,
    expert_down,
    shared_gate,
    shared_up,
    shared_down,
    exit_gain,
):
    shard_rows = query_rows.shape[0]
    head_count = key_bias.shape[1]
    head_size = query_rows.shape[1] // head_count
    ep_size = lax.axis_size("ep")
    tp_size = lax.axis_size("tp")
    row_count = routed_input.shape[0]
    local_experts = expert_gate.shape[0]
    model_width = routed_input.shape[1]
    expert_count = local_experts * ep_size
    top_count = expert_index.shape[1]
    capacity = 3 * row_count * top_count // (2 * expert_count)
    block_slots = -(-local_experts * capacity // 8) * 8
    slot_total = ep_size * block_slots
    normed = root_norm(routed_input.astype(jnp.float32), entry_gain).astype(jnp.bfloat16)
    flat_expert = expert_index.reshape(-1)
    onehot = (flat_expert[:, None] == jnp.arange(expert_count, dtype=jnp.int32)[None, :]).astype(
        jnp.int32
    )
    slot_rank = jnp.sum((jnp.cumsum(onehot, axis=0) - onehot) * onehot, axis=1)
    slot_index = (
        flat_expert // local_experts * block_slots
        + flat_expert % local_experts * capacity
        + slot_rank
    ).reshape(row_count, top_count)
    slots = jnp.arange(slot_total, dtype=jnp.int32)
    matches = slot_index[None, :, :] == slots[:, None, None]
    selector = jnp.any(matches, axis=2).astype(jnp.bfloat16)
    outgoing = jnp.dot(selector, normed, preferred_element_type=jnp.float32).astype(jnp.bfloat16)
    outgoing = outgoing.reshape(ep_size, block_slots, model_width)
    bias_rows = -(-head_count // 16) * 16
    bias_block = jnp.pad(
        jnp.transpose(key_bias),
        ((0, bias_rows - head_count), (0, 2 * key_rows.shape[1] - shard_rows)),
    )
    kv_block = jnp.concatenate(
        [jnp.concatenate([key_rows, value_rows], axis=1), bias_block], axis=0
    )
    attended, own_all, arrived = front_exchange(
        ep_size, tp_size, head_size, query_rows, kv_block, normed, outgoing
    )
    own_all = own_all.reshape(tp_size * row_count, model_width)
    mixer_term = jnp.dot(attended, mixer_weight, preferred_element_type=jnp.float32).astype(
        jnp.bfloat16
    )
    rows = arrived.reshape(tp_size * slot_total, model_width)
    tile = slot_total
    while tile > 384 and tile % 32 == 0:
        tile = tile // 2
    part = expert_parts(
        capacity, block_slots, tile, rows, expert_gate, expert_up, expert_down
    )
    part = part.reshape(tp_size, ep_size, block_slots, model_width)
    shared_term = shared_term_of(own_all, shared_gate, shared_up, shared_down).reshape(
        tp_size, row_count, model_width
    )
    mixer_term = mixer_term.reshape(tp_size, shard_rows // tp_size, model_width)
    back_rows, shared_sum, mixer_sum = back_exchange(
        ep_size, tp_size, part, shared_term, mixer_term
    )
    back_rows = back_rows.reshape(slot_total, model_width)
    placed = slot_index[:, :, None] == slots[None, None, :]
    mixing = jnp.sum(jnp.where(placed, route_weights[:, :, None], 0.0), axis=1)
    mixing_high = mixing.astype(jnp.bfloat16)
    mixing_low = (mixing - mixing_high.astype(jnp.float32)).astype(jnp.bfloat16)
    routed = jnp.dot(mixing_high, back_rows, preferred_element_type=jnp.float32) + jnp.dot(
        mixing_low, back_rows, preferred_element_type=jnp.float32
    )
    combined = routed + shared_sum
    expert_out = root_norm(combined, exit_gain).astype(jnp.bfloat16)
    mixer_out = root_norm(mixer_sum, mixer_gain).astype(jnp.bfloat16)
    return (mixer_out, expert_out)


def solution(mesh):
    in_specs = (
        P("ep", "tp"),
        P("ep", "tp"),
        P("ep", "tp"),
        P("ep", "tp"),
        P("tp", None),
        P(),
        P(("ep", "tp"), None),
        P(),
        P(("ep", "tp"), None),
        P(("ep", "tp"), None),
        P("ep", None, "tp"),
        P("ep", None, "tp"),
        P("ep", "tp", None),
        P(None, "tp"),
        P(None, "tp"),
        P("tp", None),
        P(),
    )
    out_specs = (P(("ep", "tp"), None), P(("ep", "tp"), None))
    return jax.shard_map(
        on_device, mesh=mesh, in_specs=in_specs, out_specs=out_specs, check_vma=False
    )
```

profile of v0, /device:TPU:0, one launch (start us, length us, event | category | flops | bytes accessed | tf_op | source)
XLA Modules:
  0.0 146.9 jit_solution(8811826840024425535)
XLA Ops:
  0.6 0.0 copy-start
  0.6 0.9 copy.45
  1.5 0.1 eq.50
  1.7 0.6 reduce-window.6
  2.3 0.0 copy-start.6
  2.3 0.0 copy-start.7
  2.3 0.0 copy-start.10
  2.3 0.2 slice_reduce_fusion
  2.5 0.1 bitcast_bitcast_fusion
  2.6 0.1 reduce_sum.49
  2.7 0.1 copy.48
  2.8 0.7 fusion.21
  3.5 0.1 fusion.10
  3.6 0.0 copy-start.1
  3.7 1.2 fusion.2
  4.9 1.2 fusion.4.normed_ref
  6.0 0.0 copy-start.12
  6.1 0.5 convolution_convert_fusion.1
  6.6 0.0 copy-done.6
  6.6 0.0 copy-done.7
  6.6 0.0 copy-done.10
  6.7 0.0 copy-done.1
  6.7 59.7 %front_exchange.1 = (bf16[128,256]{1,0:T(8,128)(2,1)S(1)}, bf16[4,96,2048]{2,1,0:T(8,128)(2,1)S(1)}, bf16[4,8,40,2048]{3,2,1,0:T(8,128)(2,1)}) custom-call(bf16[128,256]{1,0:T(8,128)(2,1)S(1)} %copy-done.1, bf16[144,512]{1,0:T(8,128)(2,1)S(1)} %fusion.13.kv_ref, bf16[96,2048]{1,0:T(8,128)(2,1)S(1)} %fusion.4.normed_ref, bf16[8,40,2048]{2,1,0:T(8,128)(2,1)S(1)} %bitcast.31), custom_call_target="tpu_custom_call" | custom-call | tf_op jit(solution)/shard_map/front_exchange/pallas_call | solution.py:278
  66.3 0.0 copy-done.12
  66.4 0.6 fusion.23
  66.9 0.0 copy-done
  67.0 4.2 %convolution_convert_fusion = bf16[384,2048]{1,0:T(8,128)(2,1)} fusion(bf16[256,2048]{1,0:T(8,128)(2,1)S(1)} %copy-done, bf16[384,2048]{1,0:T(8,128)(2,1)S(1)} %bitcast.33, bf16[2048,256]{1,0:T(8,128)(2,1)} %param.31, f32[384,256]{1,0:T(8,128)S(1)} %fusion.23), kind=kOutput, calls=%fused_computation | convolution fusion | flops 806682624 | bytes 5636096 | tf_op jit(solution)/shard_map/dot_general | solution.py:533
  71.1 14.0 %expert_parts.1 = bf16[1280,2048]{1,0:T(8,128)(2,1)} custom-call(bf16[1280,2048]{1,0:T(8,128)(2,1)} %bitcast.35, bf16[2,2048,256]{2,1,0:T(8,128)(2,1)} %gate_ref.1, bf16[2,2048,256]{2,1,0:T(8,128)(2,1)} %up_ref.1, bf16[2,256,2048]{2,1,0:T(8,128)(2,1)} %down_ref.1), custom_call_target="tpu_custom_call" | custom-call | tf_op jit(solution)/shard_map/expert_parts/pallas_call | solution.py:324
  85.2 0.0 copy-done.4
  85.2 1.1 convolution_convert_fusion.2
  86.3 56.1 %back_exchange.1 = (bf16[8,40,2048]{2,1,0:T(8,128)(2,1)}, f32[96,2048]{1,0:T(8,128)}, f32[32,2048]{1,0:T(8,128)}) custom-call(bf16[4,8,40,2048]{3,2,1,0:T(8,128)(2,1)} %bitcast.34, bf16[4,96,2048]{2,1,0:T(8,128)(2,1)} %bitcast.39, bf16[4,32,2048]{2,1,0:T(8,128)(2,1)} %bitcast.38), custom_call_target="tpu_custom_call" | custom-call | tf_op jit(solution)/shard_map/back_exchange/pallas_call | solution.py:487
  142.4 0.0 copy-start.2
  142.4 0.0 copy-start.5
  142.4 0.0 copy-done.11
  142.4 0.1 select_reduce_fusion
  142.5 1.9 %fusion.15 = f32[96,2048]{1,0:T(8,128)S(1)} fusion(bf16[320,2048]{1,0:T(8,128)(2,1)} %bitcast.36, f32[96,320]{1,0:T(8,128)S(1)} %select_reduce_fusion), kind=kOutput, calls=%fused_computation.31 | convolution fusion | flops 125859840 | bytes 2220032 | tf_op jit(solution)/shard_map/dot_general | solution.py:619
  144.4 0.0 copy-done.2
  144.4 0.0 copy-done.5
  144.4 0.0 copy-start.8
  144.4 0.0 copy-start.3
  144.4 0.0 copy-start.9
  144.5 0.5 multiply_reduce_fusion
  145.0 0.1 copy-done.8
  145.1 0.9 multiply_convert_fusion
  146.0 0.0 copy-done.3
  146.0 0.1 multiply_reduce_fusion.1
  146.1 0.0 copy-done.9
  146.1 0.8 multiply_convert_fusion.1
  (11 shorter events, 0.1 us)
Async XLA Ops:
  0.6 66.3 %copy-start = (bf16[256,2048]{1,0:T(8,128)(2,1)S(1)}, bf16[256,2048]{1,0:T(8,128)(2,1)}, u32[]{:S(2)}) copy-start(bf16[256,2048]{1,0:T(8,128)(2,1)} %param.32) | copy-start | bytes 3145732
  2.3 4.3 %copy-start.6 = (bf16[128,256]{1,0:T(8,128)(2,1)S(1)}, bf16[128,256]{1,0:T(8,128)(2,1)}, u32[]{:S(2)}) copy-start(bf16[128,256]{1,0:T(8,128)(2,1)} %param.19) | copy-start | bytes 196612
  2.3 4.4 %copy-start.7 = (bf16[128,256]{1,0:T(8,128)(2,1)S(1)}, bf16[128,256]{1,0:T(8,128)(2,1)}, u32[]{:S(2)}) copy-start(bf16[128,256]{1,0:T(8,128)(2,1)} %param.18) | copy-start | bytes 196612
  2.3 4.4 %copy-start.10 = (bf16[128,4]{0,1:T(4,128)(2,1)S(1)}, bf16[128,4]{0,1:T(4,128)(2,1)}, u32[]{:S(2)}) copy-start(bf16[128,4]{0,1:T(4,128)(2,1)} %param.20) | copy-start | bytes 3076
  3.6 3.0 %copy-start.1 = (bf16[128,256]{1,0:T(8,128)(2,1)S(1)}, bf16[128,256]{1,0:T(8,128)(2,1)}, u32[]{:S(2)}) copy-start(bf16[128,256]{1,0:T(8,128)(2,1)} %query_ref.1) | copy-start | bytes 196612
  6.0 60.3 %copy-start.12 = (bf16[2048,256]{1,0:T(8,128)(2,1)S(1)}, bf16[2048,256]{1,0:T(8,128)(2,1)}, u32[]{:S(2)}) copy-start(bf16[2048,256]{1,0:T(8,128)(2,1)} %param.30) | copy-start | bytes 3145732
  71.1 14.0 %copy-start.4 = (bf16[256,2048]{1,0:T(8,128)(2,1)S(1)}, bf16[256,2048]{1,0:T(8,128)(2,1)}, u32[]{:S(2)}) copy-start(bf16[256,2048]{1,0:T(8,128)(2,1)} %param.21) | copy-start | bytes 3145732
  86.3 56.1 %copy-start.11 = (f32[96,2]{0,1:T(2,128)S(1)}, f32[96,2]{0,1:T(2,128)}, u32[]{:S(2)}) copy-start(f32[96,2]{0,1:T(2,128)} %param.26) | copy-start | bytes 2308
  142.4 2.0 %copy-start.2 = (bf16[8,40,2048]{2,1,0:T(8,128)(2,1)S(1)}, bf16[8,40,2048]{2,1,0:T(8,128)(2,1)}, u32[]{:S(2)}) copy-start(bf16[8,40,2048]{2,1,0:T(8,128)(2,1)} %get-tuple-element.12) | copy-start | bytes 3932164
  142.4 2.0 %copy-start.5 = (f32[96,2048]{1,0:T(8,128)S(1)}, f32[96,2048]{1,0:T(8,128)}, u32[]{:S(2)}) copy-start(f32[96,2048]{1,0:T(8,128)} %get-tuple-element.13) | copy-start | bytes 2359300
  144.4 0.7 copy-start.8
  144.4 1.6 %copy-start.3 = (f32[32,2048]{1,0:T(8,128)S(1)}, f32[32,2048]{1,0:T(8,128)}, u32[]{:S(2)}) copy-start(f32[32,2048]{1,0:T(8,128)} %get-tuple-element.11) | copy-start | bytes 786436
  144.4 1.7 %copy-start.9 = (f32[2048]{0:T(1024)S(1)}, f32[2048]{0:T(1024)}, u32[]{:S(2)}) copy-start(f32[2048]{0:T(1024)} %param.22) | copy-start | bytes 24580
where the time goes:
time: 147 us
  Pallas kernels  130 us (88%)
  matrix products  8.81 us (6%)
  other arithmetic  5.83 us (4%)
  local copies, waits for them, and re-layouts  1.56 us (1%)
    pallas_call x1, Pallas kernels, front_exchange(): pl.pallas_call(functools.partial(front_kernel, ep_size, tp_size, head_siz...  59.7 us
    pallas_call x1, Pallas kernels, back_exchange(): pl.pallas_call(functools.partial(back_kernel, ep_size, tp_size), out_shap...  56.1 us
    pallas_call x1, Pallas kernels, expert_parts(): pl.pallas_call(functools.partial(expert_kernel, capacity, block_slots), g...  14 us
    dot_general x1, matrix products, shared_term_of(): jnp.dot(hidden, shared_down, preferred_element_type=jnp.float32)  4.17 us

commit v1 on v0

v1 whole, which is shorter than its diff:
```python
import functools

import jax
import jax.numpy as jnp
from jax import lax
from jax.experimental import pallas as pl
from jax.experimental.pallas import tpu as pltpu
from jax.sharding import PartitionSpec as P

MESH = pl.DeviceIdType.MESH
EPS = 1e-06
F32 = jnp.float32
BF16 = jnp.bfloat16


class Plan:
    def __init__(self, ep_size, tp_size, head_count, query, rows, index, gate):
        self.ep = ep_size
        self.tp = tp_size
        self.lines = ep_size // 2
        self.heads = head_count
        self.shard, self.width = query.shape
        self.head_size = self.width // head_count
        self.rows, self.model = rows.shape
        self.half = self.model // 2
        self.top = index.shape[1]
        self.local = gate.shape[0]
        self.hidden = gate.shape[2]
        self.experts = self.local * ep_size
        self.capacity = 3 * self.rows * self.top // (2 * self.experts)
        self.main = self.capacity // 16 * 16
        self.tail = self.capacity - self.main
        self.block_main = self.local * self.main
        self.block_tail = self.local * self.tail
        self.picked = self.block_main + 2 * self.block_tail
        self.block = 2 * self.block_main + 2 * self.block_tail
        self.lanes = -(-self.experts // 128) * 128
        self.padded_rows = -(-self.rows // 128) * 128


def send_of(source, target, sems, slot, place):
    return pltpu.make_async_remote_copy(
        src_ref=source,
        dst_ref=target,
        send_sem=sems[0].at[slot],
        recv_sem=sems[1].at[slot],
        device_id=place,
        device_id_type=MESH,
    )


def iota(shape, axis):
    return lax.broadcasted_iota(jnp.int32, shape, axis)


def root_norm(values, gain_row):
    return values * lax.rsqrt(jnp.mean(values * values, axis=-1, keepdims=True) + EPS) * gain_row


def silu(value):
    return value / (1.0 + jnp.exp(-value))


def tail_code(plan, place):
    row = lax.rem(place, plan.block_tail)
    return row // plan.tail * plan.capacity + plan.main + lax.rem(row, plan.tail)


def picked_code(plan, place):
    if plan.main == 0:
        return tail_code(plan, place)
    code = place // plan.main * plan.capacity + lax.rem(place, plan.main)
    if plan.tail == 0:
        return code
    after = jnp.maximum(place - plan.block_main, 0)
    return jnp.where(place < plan.block_main, code, tail_code(plan, after))


def block_code(plan, place):
    bm = plan.block_main
    if bm == 0:
        return tail_code(plan, place), place // plan.block_tail
    row = lax.rem(place, bm)
    code = row // plan.main * plan.capacity + lax.rem(row, plan.main)
    side = place // bm
    if plan.tail == 0:
        return code, side
    after = jnp.maximum(place - 2 * bm, 0)
    is_tail = place >= 2 * bm
    return (
        jnp.where(is_tail, tail_code(plan, after), code),
        jnp.where(is_tail, after // plan.block_tail, side),
    )


def layer_kernel(plan, *refs):
    (
        query_ref,
        kv_ref,
        input_ref,
        entry_ref,
        exit_ref,
        mixer_gain_ref,
        index_ref,
        route_ref,
        mixer_hbm,
        gate_hbm,
        up_hbm,
        down_hbm,
        shared_gate_hbm,
        shared_up_hbm,
        shared_down_hbm,
        mixer_out,
        expert_out,
        mixer_w,
        gate_w,
        up_w,
        down_w,
        shared_gate_w,
        shared_up_w,
        shared_down_w,
        own_all,
        info,
        info_cols,
        out,
        out_pair,
        arrived,
        part,
        near_in,
        far_out,
        far_in,
        total,
        back,
        pair_out,
        pair_in,
        shared_acc,
        shared_near,
        near_shared,
        far_shared_out,
        far_shared,
        result,
        mix_part,
        near_mix,
        far_mix_out,
        far_mix,
        kv_all,
        query_heads,
        carried,
        attended,
        weight_sem,
        own_send,
        own_recv,
        info_send,
        info_recv,
        kv_line_send,
        kv_line_recv,
        kv_pair_send,
        kv_pair_recv,
        go_send,
        go_recv,
        across_send,
        across_recv,
        partner_send,
        partner_recv,
        relay_send,
        relay_recv,
        near_send,
        near_recv,
        far_send,
        far_recv,
        return_send,
        return_recv,
        small_send,
        small_recv,
    ) = refs
    ep_size, tp_size, lines = plan.ep, plan.tp, plan.lines
    rows_n, half = plan.rows, plan.half
    bm = plan.block_main
    own_ep = lax.axis_index("ep")
    own_tp = lax.axis_index("tp")
    partner_tp = own_tp + 1 - 2 * lax.rem(own_tp, 2)
    across_tp = lax.rem(own_tp + tp_size // 2, tp_size)
    diagonal_tp = lax.rem(partner_tp + tp_size // 2, tp_size)
    line = own_ep // 2
    parity = lax.rem(own_ep, 2)
    pair_ep = own_ep + 1 - 2 * parity
    to_across = (own_ep, across_tp)
    to_partner = (own_ep, partner_tp)
    to_diagonal = (own_ep, diagonal_tp)
    to_pair = (pair_ep, own_tp)
    here = (own_ep, own_tp)

    own_sems = (own_send, own_recv)
    info_sems = (info_send, info_recv)
    kv_line_sems = (kv_line_send, kv_line_recv)
    kv_pair_sems = (kv_pair_send, kv_pair_recv)
    go_sems = (go_send, go_recv)
    across_sems = (across_send, across_recv)
    partner_sems = (partner_send, partner_recv)
    relay_sems = (relay_send, relay_recv)
    near_sems = (near_send, near_recv)
    far_sems = (far_send, far_recv)
    return_sems = (return_send, return_recv)
    small_sems = (small_send, small_recv)
    PAIR_ACROSS, PAIR_BACK, NEAR_SHARED, FAR_SHARED, NEAR_MIX, FAR_MIX = range(6)

    def to_ep(slot):
        return 2 * lax.rem(line + slot // 2, lines) + lax.rem(parity + slot, 2)

    def from_ep(slot):
        return 2 * lax.rem(line - slot // 2 + lines, lines) + lax.rem(parity + slot, 2)

    def each(first, last, action):
        lax.fori_loop(first, last, lambda step, c: (action(step), c)[1], 0)

    remote_lines = lines - 1

    def slot_of(step, side):
        return 2 * (1 + lax.rem(lines // 2 - 1 + step, max(remote_lines, 1))) + side

    barrier = pltpu.get_barrier_semaphore()

    def greet(step):
        place = lax.rem(own_ep + step, ep_size)
        pl.semaphore_signal(barrier, inc=1, device_id=(place, own_tp), device_id_type=MESH)

    each(1, ep_size, greet)
    for place in (partner_tp, across_tp, diagonal_tp):
        pl.semaphore_signal(barrier, inc=1, device_id=(own_ep, place), device_id_type=MESH)

    weights = [
        pltpu.make_async_copy(source, target, weight_sem.at[number])
        for number, (source, target) in enumerate(
            [
                (shared_gate_hbm, shared_gate_w),
                (shared_up_hbm, shared_up_w),
                (shared_down_hbm, shared_down_w),
                (gate_hbm, gate_w),
                (up_hbm, up_w),
                (down_hbm, down_w),
                (mixer_hbm, mixer_w),
            ]
        )
    ]
    for copy in weights:
        copy.start()

    normed = root_norm(input_ref[...].astype(F32), entry_ref[...]).astype(BF16)
    own_all[0] = normed

    lane = iota((rows_n, plan.lanes), 1)
    named = [lane == index_ref[:, k : k + 1] for k in range(plan.top)]
    both = jnp.zeros((rows_n, plan.lanes), F32)
    for one in named:
        both = both + jnp.where(one, 1.0, 0.0)
    earlier = jnp.where(iota((rows_n, rows_n), 0) > iota((rows_n, rows_n), 1), 1.0, 0.0)
    rank = jnp.dot(earlier.astype(BF16), both.astype(BF16), preferred_element_type=F32)
    rank = rank + lane.astype(F32) * plan.capacity
    info_lane = iota((rows_n, 128), 1)
    columns = jnp.zeros((rows_n, 128), F32)
    for k, one in enumerate(named):
        code = jnp.sum(jnp.where(one, rank, 0.0), axis=1, keepdims=True)
        columns = jnp.where(info_lane == k, code, columns)
        columns = jnp.where(info_lane == plan.top + k, route_ref[:, k : k + 1], columns)
    info_cols[...] = jnp.zeros_like(info_cols)
    info_cols[0, 0:rows_n] = columns

    def turned(value):
        return jnp.transpose(value, (1, 0))

    info[0] = turned(info_cols[0])[0:8]

    def picks(codes, rel):
        hit = codes == info[rel, 0:1, 0:rows_n]
        for k in range(1, plan.top):
            hit = hit | (codes == info[rel, k : k + 1, 0:rows_n])
        return jnp.where(hit, 1.0, 0.0).astype(BF16)

    def pack(chosen, put):
        if bm:
            put(0, bm, chosen[0:bm, 0:half])
            put(bm, 2 * bm, chosen[0:bm, half:])
        if plan.block_tail:
            side = iota((2 * plan.block_tail, half), 0) // plan.block_tail
            value = jnp.where(side == 0, chosen[bm:, 0:half], chosen[bm:, half:])
            put(2 * bm, plan.block, value)

    per_block = plan.local * plan.capacity
    picked_rows = iota((ep_size * plan.picked, 1), 0)
    picked_slot = picked_rows // plan.picked
    codes = to_ep(picked_slot) * per_block + picked_code(
        plan, lax.rem(picked_rows, plan.picked)
    )
    chosen = jnp.dot(picks(codes.astype(F32), 0), normed, preferred_element_type=F32)
    for slot in range(ep_size):

        def put_out(first, last, value, slot=slot):
            out[slot, first:last] = value.astype(BF16)

        pack(chosen[slot * plan.picked : (slot + 1) * plan.picked], put_out)

    pl.semaphore_wait(barrier, ep_size - 1 + 3)

    def own_copy(source, target, number, place):
        return send_of(own_all.at[source], own_all.at[target], own_sems, number, place)

    def info_copy(target, number, place):
        return send_of(info.at[0], info.at[target], info_sems, number, place)

    def go(slot):
        return send_of(
            out.at[slot], arrived.at[slot, 0], go_sems, slot, (to_ep(slot), own_tp)
        )

    def kv_line(source, step):
        return send_of(
            source, kv_all.at[2 * step], kv_line_sems, step, (own_ep + 2, own_tp)
        )

    def kv_pair(source, step):
        return send_of(source, kv_all.at[2 * step + 1], kv_pair_sems, step, to_pair)

    own_copy(0, 1, 0, to_across).start()
    for target, place in ((1, to_across), (2, to_partner), (3, to_diagonal)):
        info_copy(target, target, place).start()
    go(1).start()

    @pl.when(line + 1 < lines)
    def kv_first():
        kv_line(kv_ref, 1).start()

    def go_line(step):
        go(slot_of(step, 0)).start()
        go(slot_of(step, 1)).start()

    each(0, remote_lines, go_line)

    @pl.when(parity == 0)
    def kv_to_pair():
        kv_pair(kv_ref, 0).start()

    own_copy(0, 2, 1, to_partner).start()

    shard, width, heads = plan.shard, plan.width, plan.heads
    head_of = iota((shard, width), 1) // plan.head_size
    queries = query_ref[...].astype(F32) * plan.head_size ** (-0.5)
    for head in range(heads):
        query_heads[head * shard : (head + 1) * shard] = jnp.where(
            head_of == head, queries, 0.0
        ).astype(BF16)
    attended[...] = jnp.zeros_like(attended)
    carried[...] = jnp.zeros_like(carried)

    def attend_block(load, own):
        keys = load(slice(0, shard), slice(0, width))
        values = load(slice(0, shard), slice(width, 2 * width))
        bias = load(slice(shard, shard + heads), slice(0, shard)).astype(F32)
        deep = (2 * shard, 2 * shard)
        row_key, column_key = lax.rem(iota(deep, 0), shard), iota(deep, 1)
        later_of = jnp.where((row_key > column_key) | (column_key >= shard), 1.0, 0.0)
        later_of = later_of.astype(BF16)
        before = iota((shard, shard), 1) < iota((shard, shard), 0)
        scores = lax.dot_general(
            query_heads[...], keys, (((1,), (1,)), ((), ())), preferred_element_type=F32
        )
        gained = attended[...]
        for head in range(heads):
            rows = slice(head * shard, (head + 1) * shard)
            score = scores[rows] + bias[head : head + 1]
            fails = -(jnp.maximum(score, 0.0) + jnp.log(1.0 + jnp.exp(-jnp.abs(score))))
            if own:
                hits = score + fails
                fails = jnp.where(before, fails, 0.0)
            else:
                hits = score + fails
            high = fails.astype(BF16)
            low = (fails - high.astype(F32)).astype(BF16)
            sums = jnp.dot(
                jnp.concatenate([high, low], axis=1), later_of, preferred_element_type=F32
            )
            taken = carried[rows]
            weights = jnp.exp(hits + sums[:, 0:shard] + taken)
            if own:
                weights = jnp.where(before, weights, 0.0)
            product = jnp.dot(weights.astype(BF16), values, preferred_element_type=F32)
            gained = gained + jnp.where(head_of == head, product, 0.0)
            carried[rows] = taken + sums[:, shard : 2 * shard]
        attended[...] = gained

    attend_block(lambda rows, cols: kv_ref[rows, cols], True)

    def attend_slot(slot):
        attend_block(lambda rows, cols: kv_all[slot, rows, cols], False)

    def kv_step(step):
        @pl.when(step <= line)
        def one():
            block = kv_all.at[2 * step]
            send_of(block, block, kv_line_sems, step, here).wait_recv()

            @pl.when(line + 1 < lines)
            def further():
                kv_line(block, step + 1).start()

            kv_pair(block, step).start()

    def attend_step(step):
        @pl.when(step <= line)
        def one():
            other = kv_all.at[2 * step + 1]
            send_of(other, other, kv_pair_sems, step, here).wait_recv()

            def turn(side, c):
                attend_slot(2 * step + lax.rem(side + 1 - parity, 2))
                return c

            lax.fori_loop(0, 2, turn, 0)

    def landed(slot):
        block = arrived.at[slot, 0]
        return send_of(block, block, go_sems, slot, here)

    def to_side(rel, slot, target, sems, place):
        return send_of(arrived.at[slot, rel], arrived.at[slot, target], sems, slot, place)

    landed(1).wait_recv()
    to_side(0, 1, 2, partner_sems, to_partner).start()

    own_copy(1, 1, 0, here).wait_recv()
    own_copy(1, 3, 2, to_partner).start()
    info_copy(1, 1, here).wait_recv()

    def choose(target_ep, rel, put):
        place = iota((plan.picked, 1), 0)
        codes = target_ep * per_block + picked_code(plan, place)
        pack(
            jnp.dot(picks(codes.astype(F32), rel), own_all[rel], preferred_element_type=F32), put
        )

    def put_pair(first, last, value):
        out_pair[first:last] = value.astype(BF16)

    choose(pair_ep, 1, put_pair)
    pair_across = send_of(out_pair, arrived.at[1, 1], small_sems, PAIR_ACROSS, to_pair)
    pair_across.start()

    @pl.when(parity == 1)
    def attend_pair():
        block = kv_all.at[1]
        send_of(block, block, kv_pair_sems, 0, here).wait_recv()
        attend_slot(1)

    def forward(step):
        for side in range(2):
            slot = slot_of(step, side)
            landed(slot).wait_recv()
            to_side(0, slot, 1, across_sems, to_across).start()
            to_side(0, slot, 2, partner_sems, to_partner).start()

    if remote_lines:
        forward(0)
        kv_step(1)

    own_copy(2, 2, 1, here).wait_recv()
    own_copy(3, 3, 2, here).wait_recv()
    for rel in (2, 3):
        info_copy(rel, rel, here).wait_recv()
    for rel in (1, 2, 3):
        info_cols[rel, :, 0:8] = turned(info[rel])
    for copy in weights[0:3]:
        copy.wait()
    shared_rows = own_all[...].reshape(tp_size * rows_n, plan.model)
    hidden = silu(jnp.dot(shared_rows, shared_gate_w[...], preferred_element_type=F32))
    hidden = hidden * jnp.dot(shared_rows, shared_up_w[...], preferred_element_type=F32)
    shared_acc[...] = jnp.dot(
        hidden.astype(BF16), shared_down_w[...], preferred_element_type=F32
    ).reshape(shared_acc.shape)

    def put_own(first, last, value, rel):
        arrived[0, rel, first:last] = value.astype(BF16)

    arrived[0, 0] = out[0]
    for rel in (1, 2, 3):
        choose(own_ep, rel, functools.partial(put_own, rel=rel))

    blocks = 2 * tp_size
    tails = blocks * plan.tail
    folded = blocks * 2 * plan.block_tail

    def tail_move(side, by_column):
        shape = (folded, plan.local * tails) if by_column else (plan.local * tails, folded)
        sorted_at = iota(shape, 1 if by_column else 0)
        folded_at = iota(shape, 0 if by_column else 1)
        expert = sorted_at // tails
        block = lax.rem(sorted_at, tails) // plan.tail
        spot = lax.rem(sorted_at, plan.tail)
        target = (
            block * 2 * plan.block_tail + side * plan.block_tail + expert * plan.tail + spot
        )
        return jnp.where(folded_at == target, 1.0, 0.0).astype(BF16)

    def experts(first):
        pair = arrived.at[pl.ds(first, 2)]
        tail_rows = None
        if plan.tail:
            folded_rows = pair[:, :, 2 * bm : plan.block].reshape(folded, half)
            tail_rows = jnp.concatenate(
                [
                    jnp.dot(tail_move(side, False), folded_rows, preferred_element_type=F32)
                    for side in range(2)
                ],
                axis=1,
            ).astype(BF16)
        tail_results = []
        for expert in range(plan.local):
            pieces = []
            if plan.main:
                at = expert * plan.main
                left = pair[:, :, at : at + plan.main]
                right = pair[:, :, bm + at : bm + at + plan.main]
                pieces.append(
                    jnp.concatenate([left, right], axis=3).reshape(
                        blocks * plan.main, plan.model
                    )
                )
            if plan.tail:
                pieces.append(tail_rows[expert * tails : (expert + 1) * tails])
            x = pieces[0] if len(pieces) == 1 else jnp.concatenate(pieces, axis=0)
            hidden = silu(jnp.dot(x, gate_w[expert], preferred_element_type=F32))
            hidden = hidden * jnp.dot(x, up_w[expert], preferred_element_type=F32)
            result_rows = jnp.dot(
                hidden.astype(BF16), down_w[expert], preferred_element_type=F32
            ).astype(BF16)
            if plan.main:
                at = expert * plan.main
                shape = (2, tp_size, plan.main, half)
                count = blocks * plan.main
                part[pl.ds(first, 2), :, at : at + plan.main] = result_rows[
                    0:count, 0:half
                ].reshape(shape)
                part[pl.ds(first, 2), :, bm + at : bm + at + plan.main] = result_rows[
                    0:count, half:
                ].reshape(shape)
            if plan.tail:
                tail_results.append(result_rows[blocks * plan.main :])
        if plan.tail:
            ends = jnp.concatenate(tail_results, axis=0)
            value = jnp.dot(
                tail_move(0, True), ends[:, 0:half], preferred_element_type=F32
            ) + jnp.dot(tail_move(1, True), ends[:, half:], preferred_element_type=F32)
            part[pl.ds(first, 2), :, 2 * bm : plan.block] = value.astype(BF16).reshape(
                2, tp_size, 2 * plan.block_tail, half
            )

    def mixed(target_ep, rel, load):
        place = iota((1, plan.block), 1)
        code, side = block_code(plan, place)
        code = (code + target_ep * per_block).astype(F32)
        weight = jnp.zeros((rows_n, plan.block), F32)
        for k in range(plan.top):
            hit = code == info_cols[rel, 0:rows_n, k : k + 1]
            at = plan.top + k
            weight = weight + jnp.where(hit, info_cols[rel, 0:rows_n, at : at + 1], 0.0)
        sums = []
        for which in range(2):
            kept = jnp.where(side == which, weight, 0.0)
            high = kept.astype(BF16)
            low = (kept - high.astype(F32)).astype(BF16)
            value = jnp.dot(
                jnp.concatenate([high, low], axis=0), load(), preferred_element_type=F32
            )
            sums.append(value[0:rows_n] + value[rows_n:])
        return jnp.concatenate(sums, axis=1)

    def near(slot):
        return send_of(
            part.at[slot, pl.ds(2, 2)], near_in.at[slot], near_sems, slot, to_partner
        )

    block = arrived.at[1, 1]
    send_of(block, block, small_sems, PAIR_ACROSS, here).wait_recv()
    to_side(1, 1, 3, relay_sems, to_partner).start()
    to_side(2, 1, 2, partner_sems, here).wait_recv()
    to_side(3, 1, 3, relay_sems, here).wait_recv()
    for copy in weights[3:6]:
        copy.wait()
    experts(0)
    near(1).start()
    for rel in range(tp_size):
        shared_acc[rel] = shared_acc[rel] + mixed(own_ep, rel, lambda rel=rel: part[0, rel])
    shared_near[...] = shared_acc[2:4].astype(BF16)
    shared_near_copy = send_of(shared_near, near_shared, small_sems, NEAR_SHARED, to_partner)
    shared_near_copy.start()
    near(1).wait_recv()
    pair_out[...] = (part[1, 0:2].astype(F32) + near_in[1].astype(F32)).astype(BF16)
    pair_back = send_of(pair_out, pair_in, small_sems, PAIR_BACK, to_pair)
    pair_back.start()

    def relay(step):
        for side in range(2):
            slot = slot_of(step, side)
            to_side(1, slot, 1, across_sems, here).wait_recv()
            to_side(1, slot, 3, relay_sems, to_partner).start()

    def ready(step):
        for side in range(2):
            slot = slot_of(step, side)
            to_side(2, slot, 2, partner_sems, here).wait_recv()
            to_side(3, slot, 3, relay_sems, here).wait_recv()

    def far(slot):
        return send_of(far_out.at[slot], far_in.at[slot], far_sems, slot, to_across)

    def send_far(step):
        for side in range(2):
            slot = slot_of(step, side)
            near(slot).wait_recv()
            far_out[slot] = (part[slot, 1].astype(F32) + near_in[slot, 1].astype(F32)).astype(
                BF16
            )
            far(slot).start()

    def give_back(slot):
        return send_of(
            total.at[slot], back.at[slot], return_sems, slot, (from_ep(slot), own_tp)
        )

    def send_total(step):
        for side in range(2):
            slot = slot_of(step, side)
            far(slot).wait_recv()
            total[slot] = (
                part[slot, 0].astype(F32)
                + near_in[slot, 0].astype(F32)
                + far_in[slot].astype(F32)
            ).astype(BF16)
            give_back(slot).start()

    def turn(step):
        @pl.when((step >= 1) & (step < remote_lines))
        def next_line():
            forward(step)
            kv_step(step + 1)

        @pl.when(step < remote_lines)
        def attend_line():
            attend_step(step + 1)

        @pl.when((step >= 1) & (step <= remote_lines))
        def compute():
            relay(step - 1)
            ready(step - 1)
            experts(slot_of(step - 1, 0))
            for side in range(2):
                near(slot_of(step - 1, side)).start()

        @pl.when(step >= 2)
        def answer():
            send_total(step - 2)

        @pl.when((step >= 1) & (step <= remote_lines))
        def reduce_far():
            send_far(step - 1)

    if remote_lines:
        each(0, remote_lines + 2, turn)

    weights[6].wait()
    rows_out = shard // tp_size
    mixer_term = jnp.dot(
        attended[...].astype(BF16), mixer_w[...], preferred_element_type=F32
    ).astype(BF16)
    for place in range(tp_size):
        high = lax.rem(place // 2 + own_tp // 2, 2)
        low = lax.rem(place + own_tp, 2)
        mix_part[high + 2 * low] = mixer_term[place * rows_out : (place + 1) * rows_out]
    mix_near_copy = send_of(
        mix_part.at[pl.ds(2, 2)], near_mix, small_sems, NEAR_MIX, to_partner
    )
    mix_near_copy.start()

    shared_near_copy.wait_recv()
    pair_back.wait_recv()
    far_shared_out[...] = (
        shared_acc[1] + near_shared[1].astype(F32) + mixed(pair_ep, 1, lambda: pair_in[1])
    ).astype(BF16)
    shared_far_copy = send_of(far_shared_out, far_shared, small_sems, FAR_SHARED, to_across)
    shared_far_copy.start()
    mix_near_copy.wait_recv()
    far_mix_out[...] = (mix_part[1].astype(F32) + near_mix[1].astype(F32)).astype(BF16)
    mix_far_copy = send_of(far_mix_out, far_mix, small_sems, FAR_MIX, to_across)
    mix_far_copy.start()
    result[...] = (
        shared_acc[0] + near_shared[0].astype(F32) + mixed(pair_ep, 0, lambda: pair_in[0])
    )

    def take_back(step):
        for side in range(2):
            slot = slot_of(step, side)
            block = back.at[slot]
            send_of(block, block, return_sems, slot, here).wait_recv()
            result[...] = result[...] + mixed(to_ep(slot), 0, lambda: back[slot])

    each(0, remote_lines, take_back)
    shared_far_copy.wait_recv()
    combined = result[...] + far_shared[...].astype(F32)
    expert_out[...] = root_norm(combined, exit_ref[...]).astype(BF16)
    mix_far_copy.wait_recv()
    mixer_sum = (
        mix_part[0].astype(F32) + near_mix[0].astype(F32) + far_mix[...].astype(F32)
    )
    mixer_out[...] = root_norm(mixer_sum, mixer_gain_ref[...]).astype(BF16)

    own_copy(0, 1, 0, to_across).wait_send()
    own_copy(0, 2, 1, to_partner).wait_send()
    own_copy(1, 3, 2, to_partner).wait_send()
    for target, place in ((1, to_across), (2, to_partner), (3, to_diagonal)):
        info_copy(target, target, place).wait_send()
    go(1).wait_send()
    to_side(0, 1, 2, partner_sems, to_partner).wait_send()
    to_side(1, 1, 3, relay_sems, to_partner).wait_send()
    near(1).wait_send()
    for copy in (
        pair_across,
        pair_back,
        shared_near_copy,
        shared_far_copy,
        mix_near_copy,
        mix_far_copy,
    ):
        copy.wait_send()

    def finish(slot):
        go(slot).wait_send()
        to_side(0, slot, 1, across_sems, to_across).wait_send()
        to_side(0, slot, 2, partner_sems, to_partner).wait_send()
        to_side(1, slot, 3, relay_sems, to_partner).wait_send()
        near(slot).wait_send()
        far(slot).wait_send()
        give_back(slot).wait_send()

    each(2, ep_size, finish)

    def finish_kv(step):
        @pl.when((step <= line) & (line + 1 < lines))
        def sent_on():
            kv_line(kv_all.at[2 * step], step + 1).wait_send()

        @pl.when((step <= line) & (step >= 1))
        def sent_over():
            kv_pair(kv_all.at[2 * step], step).wait_send()

    each(0, lines, finish_kv)

    @pl.when(parity == 0)
    def sent_pair():
        kv_pair(kv_ref, 0).wait_send()


def on_device(
    query_rows,
    key_rows,
    value_rows,
    key_bias,
    mixer_weight,
    mixer_gain,
    routed_input,
    entry_gain,
    expert_index,
    route_weights,
    expert_gate,
    expert_up,
    expert_down,
    shared_gate,
    shared_up,
    shared_down,
    exit_gain,
):
    ep_size = lax.axis_size("ep")
    tp_size = lax.axis_size("tp")
    plan = Plan(
        ep_size, tp_size, key_bias.shape[1], query_rows, routed_input, expert_index, expert_gate
    )
    shard, width, model, rows = plan.shard, plan.width, plan.model, plan.rows
    bias_rows = -(-plan.heads // 16) * 16
    bias_block = jnp.pad(
        jnp.transpose(key_bias), ((0, bias_rows - plan.heads), (0, 2 * width - shard))
    )
    kv_block = jnp.concatenate(
        [jnp.concatenate([key_rows, value_rows], axis=1), bias_block], axis=0
    )
    small = [
        query_rows,
        kv_block,
        routed_input,
        entry_gain.reshape(1, model),
        exit_gain.reshape(1, model),
        mixer_gain.reshape(1, model),
        expert_index,
        route_weights,
    ]
    large = [
        mixer_weight,
        expert_gate,
        expert_up,
        expert_down,
        shared_gate,
        shared_up,
        shared_down,
    ]
    vmem = pl.BlockSpec(memory_space=pltpu.VMEM)
    block = (plan.block, plan.half)
    mix = (shard // tp_size, model)

    def buffer(*shape, kind=BF16):
        return pltpu.VMEM(shape, kind)

    scratch = [pltpu.VMEM(value.shape, value.dtype) for value in large]
    scratch += [
        buffer(tp_size, rows, model),
        buffer(tp_size, 8, plan.padded_rows, kind=F32),
        buffer(tp_size, plan.padded_rows, 128, kind=F32),
        buffer(ep_size, *block),
        buffer(*block),
        buffer(ep_size, tp_size, *block),
        buffer(ep_size, tp_size, *block),
        buffer(ep_size, 2, *block),
        buffer(ep_size, *block),
        buffer(ep_size, *block),
        buffer(ep_size, *block),
        buffer(ep_size, *block),
        buffer(2, *block),
        buffer(2, *block),
        buffer(tp_size, rows, model, kind=F32),
        buffer(2, rows, model),
        buffer(2, rows, model),
        buffer(rows, model),
        buffer(rows, model),
        buffer(rows, model, kind=F32),
        buffer(tp_size, *mix),
        buffer(2, *mix),
        buffer(*mix),
        buffer(*mix),
        buffer(ep_size, *kv_block.shape),
        buffer(plan.heads * shard, width),
        buffer(plan.heads * shard, shard, kind=F32),
        buffer(shard, width, kind=F32),
    ]
    sem = pltpu.SemaphoreType.DMA
    scratch += [sem((len(large),))]
    for count in (4, 4, ep_size, ep_size, ep_size, ep_size, ep_size, ep_size, ep_size, ep_size, ep_size, 6):
        scratch += [sem((count,)), sem((count,))]
    mixer_out, expert_out = pl.pallas_call(
        functools.partial(layer_kernel, plan),
        out_shape=(
            jax.ShapeDtypeStruct(mix, BF16),
            jax.ShapeDtypeStruct((rows, model), BF16),
        ),
        in_specs=[vmem] * len(small) + [pl.BlockSpec(memory_space=pl.ANY)] * len(large),
        out_specs=(vmem, vmem),
        scratch_shapes=scratch,
        compiler_params=pltpu.CompilerParams(
            collective_id=0, has_side_effects=True, vmem_limit_bytes=62 * 1024 * 1024
        ),
        name="whole_layer",
    )(*small, *large)
    return (mixer_out, expert_out)


def solution(mesh):
    in_specs = (
        P("ep", "tp"),
        P("ep", "tp"),
        P("ep", "tp"),
        P("ep", "tp"),
        P("tp", None),
        P(),
        P(("ep", "tp"), None),
        P(),
        P(("ep", "tp"), None),
        P(("ep", "tp"), None),
        P("ep", None, "tp"),
        P("ep", None, "tp"),
        P("ep", "tp", None),
        P(None, "tp"),
        P(None, "tp"),
        P("tp", None),
        P(),
    )
    out_specs = (P(("ep", "tp"), None), P(("ep", "tp"), None))
    return jax.shard_map(
        on_device, mesh=mesh, in_specs=in_specs, out_specs=out_specs, check_vma=False
    )
```

time: 147 us -> 103 us (0.70)
  the two profiles are of different devices: /device:TPU:0 before, /device:TPU:24 now
where the time goes in v1:
time: 103 us
  Pallas kernels  94.9 us (92%)
  local copies, waits for them, and re-layouts  6.12 us (6%)
  other arithmetic  1.56 us (2%)
    pallas_call x1, Pallas kernels, on_device(): pl.pallas_call(functools.partial(layer_kernel, plan), out_shape=(jax.Shap...  94.9 us
    unnamed x4, local copies, waits for them, and re-layouts  6.12 us

profile of v1, /device:TPU:24, one launch (start us, length us, event | category | flops | bytes accessed | tf_op | source)
XLA Modules:
  0.0 103.2 jit_solution(3981767696601032834)
XLA Ops:
  0.6 1.4 %copy.19.refs_6_ = s32[96,2]{1,0:T(8,128)} copy(s32[96,2]{0,1:T(2,128)} %param.25) | data formatting | bytes 1536 | tf_op args[8]
  2.0 1.4 %copy.20.refs_7_ = f32[96,2]{1,0:T(8,128)} copy(f32[96,2]{0,1:T(2,128)} %param.26) | data formatting | bytes 1536 | tf_op args[9]
  3.4 1.6 %fusion.1.refs_1_ = bf16[144,512]{1,0:T(8,128)(2,1)} fusion(bf16[4,128]{1,0:T(4,128)(2,1)} %bitcast.7, bf16[128,256]{1,0:T(8,128)(2,1)} %param.19, bf16[128,256]{1,0:T(8,128)(2,1)} %param.18), kind=kLoop, calls=%fused_computation.2 | loop fusion | flops 589824 | bytes 279552 | tf_op jit(solution)/shard_map/concatenate | solution.py:789
  5.0 94.9 %whole_layer.1 = (bf16[32,2048]{1,0:T(8,128)(2,1)}, bf16[96,2048]{1,0:T(8,128)(2,1)}) custom-call(bf16[128,256]{1,0:T(8,128)(2,1)} %refs_0_.1, bf16[144,512]{1,0:T(8,128)(2,1)} %fusion.1.refs_1_, bf16[96,2048]{1,0:T(8,128)(2,1)} %refs_2_.1, f32[1,2048]{1,0:T(1,128)} %bitcast.4, f32[1,2048]{1,0:T(1,128)} %bitcast.5, f32[1,2048]{1,0:T(1,128)} %bitcast.6, ...), custom_call_target="tpu_custom_call" | custom-call | tf_op jit(solution)/shard_map/whole_layer/pallas_call | solution.py:853
  99.8 1.6 %copy.23 = bf16[32,2048]{1,0:T(8,128)(2,1)} copy(bf16[32,2048]{1,0:T(8,128)(2,1)} %get-tuple-element.4) | data formatting | bytes 262144
  101.4 1.8 %copy.24 = bf16[96,2048]{1,0:T(8,128)(2,1)} copy(bf16[96,2048]{1,0:T(8,128)(2,1)} %get-tuple-element.5) | data formatting | bytes 786432

commit v2 on v1

--- a/solution.py
+++ b/solution.py
@@ -34,7 +34,7 @@
         self.block_tail = self.local * self.tail
         self.picked = self.block_main + 2 * self.block_tail
         self.block = 2 * self.block_main + 2 * self.block_tail
-        self.lanes = -(-self.experts // 128) * 128
+        self.named = -(-self.experts // 16) * 16
         self.padded_rows = -(-self.rows // 128) * 128
 
 
@@ -47,6 +47,16 @@
         device_id=place,
         device_id_type=MESH,
     )
+
+
+def got(name, copy):
+    with jax.named_scope(name):
+        copy.wait_recv()
+
+
+def timed(name, action, *args):
+    with jax.named_scope(name):
+        return action(*args)
 
 
 def iota(shape, axis):
@@ -96,11 +106,11 @@
 def layer_kernel(plan, *refs):
     (
         query_ref,
-        kv_ref,
+        key_ref,
+        value_ref,
+        bias_ref,
         input_ref,
         entry_ref,
-        exit_ref,
-        mixer_gain_ref,
         index_ref,
         route_ref,
         mixer_hbm,
@@ -143,6 +153,7 @@
         near_mix,
         far_mix_out,
         far_mix,
+        kv_ref,
         kv_all,
         query_heads,
         carried,
@@ -215,8 +226,22 @@
 
     remote_lines = lines - 1
 
+    def other_line(step):
+        middle = lines // 2
+        inner = jnp.minimum(line, lines - 1 - line)
+        index = jnp.where(step <= middle + inner - 1, step - 1, step)
+        around = index < 2 * inner
+        distance = jnp.where(around, index // 2 + 1, index - inner + 1)
+        to_end = jnp.where(around, lax.rem(index, 2), 1)
+        upward = (2 * line < lines) == (to_end == 1)
+        near_line = jnp.where(upward, line + distance, line - distance)
+        return jnp.where(step == 0, lax.rem(line + middle, lines), near_line)
+
     def slot_of(step, side):
-        return 2 * (1 + lax.rem(lines // 2 - 1 + step, max(remote_lines, 1))) + side
+        return 2 * lax.rem(line - other_line(step) + lines, lines) + side
+
+    def slot_to(step, side):
+        return 2 * lax.rem(other_line(step) - line + lines, lines) + side
 
     barrier = pltpu.get_barrier_semaphore()
 
@@ -248,27 +273,31 @@
     normed = root_norm(input_ref[...].astype(F32), entry_ref[...]).astype(BF16)
     own_all[0] = normed
 
-    lane = iota((rows_n, plan.lanes), 1)
-    named = [lane == index_ref[:, k : k + 1] for k in range(plan.top)]
-    both = jnp.zeros((rows_n, plan.lanes), F32)
+    with jax.named_scope("wait_barrier"):
+        pl.semaphore_wait(barrier, ep_size - 1 + 3)
+
+    def own_copy(source, target, number, place):
+        return send_of(own_all.at[source], own_all.at[target], own_sems, number, place)
+
+    own_copy(0, 1, 0, to_across).start()
+    own_copy(0, 2, 1, to_partner).start()
+
+    expert_at = iota((plan.named, rows_n), 0)
+    named = [expert_at == index_ref[k : k + 1] for k in range(plan.top)]
+    both = jnp.zeros((plan.named, rows_n), F32)
     for one in named:
         both = both + jnp.where(one, 1.0, 0.0)
-    earlier = jnp.where(iota((rows_n, rows_n), 0) > iota((rows_n, rows_n), 1), 1.0, 0.0)
-    rank = jnp.dot(earlier.astype(BF16), both.astype(BF16), preferred_element_type=F32)
-    rank = rank + lane.astype(F32) * plan.capacity
-    info_lane = iota((rows_n, 128), 1)
-    columns = jnp.zeros((rows_n, 128), F32)
+    earlier = jnp.where(iota((rows_n, rows_n), 0) < iota((rows_n, rows_n), 1), 1.0, 0.0)
+    rank = jnp.dot(both.astype(BF16), earlier.astype(BF16), preferred_element_type=F32)
+    rank = rank + expert_at.astype(F32) * plan.capacity
+    info[0] = jnp.zeros_like(info[0])
     for k, one in enumerate(named):
-        code = jnp.sum(jnp.where(one, rank, 0.0), axis=1, keepdims=True)
-        columns = jnp.where(info_lane == k, code, columns)
-        columns = jnp.where(info_lane == plan.top + k, route_ref[:, k : k + 1], columns)
-    info_cols[...] = jnp.zeros_like(info_cols)
-    info_cols[0, 0:rows_n] = columns
+        code = jnp.sum(jnp.where(one, rank, 0.0), axis=0, keepdims=True)
+        info[0, k : k + 1, 0:rows_n] = code
+        info[0, plan.top + k : plan.top + k + 1, 0:rows_n] = route_ref[k : k + 1]
 
     def turned(value):
         return jnp.transpose(value, (1, 0))
-
-    info[0] = turned(info_cols[0])[0:8]
 
     def picks(codes, rel):
         hit = codes == info[rel, 0:1, 0:rows_n]
@@ -299,10 +328,11 @@
 
         pack(chosen[slot * plan.picked : (slot + 1) * plan.picked], put_out)
 
-    pl.semaphore_wait(barrier, ep_size - 1 + 3)
-
-    def own_copy(source, target, number, place):
-        return send_of(own_all.at[source], own_all.at[target], own_sems, number, place)
+    shard, width, heads = plan.shard, plan.width, plan.heads
+    kv_ref[0:shard, 0:width] = key_ref[...]
+    kv_ref[0:shard, width:] = value_ref[...]
+    kv_ref[shard:] = jnp.zeros((kv_ref.shape[0] - shard, 2 * width), BF16)
+    kv_ref[shard : shard + heads, 0:shard] = bias_ref[...]
 
     def info_copy(target, number, place):
         return send_of(info.at[0], info.at[target], info_sems, number, place)
@@ -320,28 +350,27 @@
     def kv_pair(source, step):
         return send_of(source, kv_all.at[2 * step + 1], kv_pair_sems, step, to_pair)
 
-    own_copy(0, 1, 0, to_across).start()
     for target, place in ((1, to_across), (2, to_partner), (3, to_diagonal)):
         info_copy(target, target, place).start()
     go(1).start()
 
+    def go_line(step):
+        go(slot_to(step, 0)).start()
+        go(slot_to(step, 1)).start()
+
+    early = max(remote_lines - 1, 0)
+    each(0, early, go_line)
+
     @pl.when(line + 1 < lines)
     def kv_first():
         kv_line(kv_ref, 1).start()
 
-    def go_line(step):
-        go(slot_of(step, 0)).start()
-        go(slot_of(step, 1)).start()
-
-    each(0, remote_lines, go_line)
+    each(early, remote_lines, go_line)
 
     @pl.when(parity == 0)
     def kv_to_pair():
         kv_pair(kv_ref, 0).start()
 
-    own_copy(0, 2, 1, to_partner).start()
-
-    shard, width, heads = plan.shard, plan.width, plan.heads
     head_of = iota((shard, width), 1) // plan.head_size
     queries = query_ref[...].astype(F32) * plan.head_size ** (-0.5)
     for head in range(heads):
@@ -387,7 +416,7 @@
             carried[rows] = taken + sums[:, shard : 2 * shard]
         attended[...] = gained
 
-    attend_block(lambda rows, cols: kv_ref[rows, cols], True)
+    timed("attend_own", attend_block, lambda rows, cols: kv_ref[rows, cols], True)
 
     def attend_slot(slot):
         attend_block(lambda rows, cols: kv_all[slot, rows, cols], False)
@@ -396,7 +425,7 @@
         @pl.when(step <= line)
         def one():
             block = kv_all.at[2 * step]
-            send_of(block, block, kv_line_sems, step, here).wait_recv()
+            got("wait_kv_line", send_of(block, block, kv_line_sems, step, here))
 
             @pl.when(line + 1 < lines)
             def further():
@@ -408,10 +437,10 @@
         @pl.when(step <= line)
         def one():
             other = kv_all.at[2 * step + 1]
-            send_of(other, other, kv_pair_sems, step, here).wait_recv()
+            got("wait_kv_pair", send_of(other, other, kv_pair_sems, step, here))
 
             def turn(side, c):
-                attend_slot(2 * step + lax.rem(side + 1 - parity, 2))
+                timed("attend", attend_slot, 2 * step + lax.rem(side + 1 - parity, 2))
                 return c
 
             lax.fori_loop(0, 2, turn, 0)
@@ -423,10 +452,10 @@
     def to_side(rel, slot, target, sems, place):
         return send_of(arrived.at[slot, rel], arrived.at[slot, target], sems, slot, place)
 
-    landed(1).wait_recv()
+    got("wait_pair", landed(1))
     to_side(0, 1, 2, partner_sems, to_partner).start()
 
-    own_copy(1, 1, 0, here).wait_recv()
+    got("wait_own_across", own_copy(1, 1, 0, here))
     own_copy(1, 3, 2, to_partner).start()
     info_copy(1, 1, here).wait_recv()
 
@@ -444,44 +473,49 @@
     pair_across = send_of(out_pair, arrived.at[1, 1], small_sems, PAIR_ACROSS, to_pair)
     pair_across.start()
 
-    @pl.when(parity == 1)
-    def attend_pair():
-        block = kv_all.at[1]
-        send_of(block, block, kv_pair_sems, 0, here).wait_recv()
-        attend_slot(1)
+    def forward_side(step, side):
+        slot = slot_of(step, side)
+        got("wait_landed", landed(slot))
+        to_side(0, slot, 1, across_sems, to_across).start()
+        to_side(0, slot, 2, partner_sems, to_partner).start()
 
     def forward(step):
         for side in range(2):
-            slot = slot_of(step, side)
-            landed(slot).wait_recv()
-            to_side(0, slot, 1, across_sems, to_across).start()
-            to_side(0, slot, 2, partner_sems, to_partner).start()
+            forward_side(step, side)
 
     if remote_lines:
-        forward(0)
-        kv_step(1)
-
-    own_copy(2, 2, 1, here).wait_recv()
-    own_copy(3, 3, 2, here).wait_recv()
+        forward_side(0, 0)
+
+    got("wait_own_partner", own_copy(2, 2, 1, here))
+    got("wait_own_diag", own_copy(3, 3, 2, here))
     for rel in (2, 3):
         info_copy(rel, rel, here).wait_recv()
-    for rel in (1, 2, 3):
+    for rel in range(tp_size):
         info_cols[rel, :, 0:8] = turned(info[rel])
     for copy in weights[0:3]:
         copy.wait()
-    shared_rows = own_all[...].reshape(tp_size * rows_n, plan.model)
-    hidden = silu(jnp.dot(shared_rows, shared_gate_w[...], preferred_element_type=F32))
-    hidden = hidden * jnp.dot(shared_rows, shared_up_w[...], preferred_element_type=F32)
-    shared_acc[...] = jnp.dot(
-        hidden.astype(BF16), shared_down_w[...], preferred_element_type=F32
-    ).reshape(shared_acc.shape)
+
+    def shared_expert():
+        shared_rows = own_all[...].reshape(tp_size * rows_n, plan.model)
+        hidden = silu(jnp.dot(shared_rows, shared_gate_w[...], preferred_element_type=F32))
+        hidden = hidden * jnp.dot(shared_rows, shared_up_w[...], preferred_element_type=F32)
+        shared_acc[...] = jnp.dot(
+            hidden.astype(BF16), shared_down_w[...], preferred_element_type=F32
+        ).reshape(shared_acc.shape)
+
+    timed("shared", shared_expert)
+    if remote_lines:
+        forward_side(0, 1)
 
     def put_own(first, last, value, rel):
         arrived[0, rel, first:last] = value.astype(BF16)
 
-    arrived[0, 0] = out[0]
-    for rel in (1, 2, 3):
-        choose(own_ep, rel, functools.partial(put_own, rel=rel))
+    def choose_own():
+        arrived[0, 0] = out[0]
+        for rel in (1, 2, 3):
+            choose(own_ep, rel, functools.partial(put_own, rel=rel))
+
+    timed("choose_own", choose_own)
 
     blocks = 2 * tp_size
     tails = blocks * plan.tail
@@ -578,35 +612,47 @@
         )
 
     block = arrived.at[1, 1]
-    send_of(block, block, small_sems, PAIR_ACROSS, here).wait_recv()
+    got("wait_pair_across", send_of(block, block, small_sems, PAIR_ACROSS, here))
     to_side(1, 1, 3, relay_sems, to_partner).start()
-    to_side(2, 1, 2, partner_sems, here).wait_recv()
-    to_side(3, 1, 3, relay_sems, here).wait_recv()
+    got("wait_pair_p", to_side(2, 1, 2, partner_sems, here))
+    got("wait_pair_r", to_side(3, 1, 3, relay_sems, here))
     for copy in weights[3:6]:
         copy.wait()
-    experts(0)
+    timed("experts_own", experts, 0)
     near(1).start()
-    for rel in range(tp_size):
-        shared_acc[rel] = shared_acc[rel] + mixed(own_ep, rel, lambda rel=rel: part[0, rel])
+    if remote_lines > 1:
+        forward(1)
+
+    def fold_own():
+        for rel in range(tp_size):
+            shared_acc[rel] = shared_acc[rel] + mixed(own_ep, rel, lambda rel=rel: part[0, rel])
+
+    timed("fold_own", fold_own)
     shared_near[...] = shared_acc[2:4].astype(BF16)
     shared_near_copy = send_of(shared_near, near_shared, small_sems, NEAR_SHARED, to_partner)
     shared_near_copy.start()
-    near(1).wait_recv()
+    got("wait_near1", near(1))
     pair_out[...] = (part[1, 0:2].astype(F32) + near_in[1].astype(F32)).astype(BF16)
     pair_back = send_of(pair_out, pair_in, small_sems, PAIR_BACK, to_pair)
     pair_back.start()
 
+    @pl.when(parity == 1)
+    def attend_pair():
+        block = kv_all.at[1]
+        got("wait_kv_pair", send_of(block, block, kv_pair_sems, 0, here))
+        timed("attend", attend_slot, 1)
+
     def relay(step):
         for side in range(2):
             slot = slot_of(step, side)
-            to_side(1, slot, 1, across_sems, here).wait_recv()
+            got("wait_across", to_side(1, slot, 1, across_sems, here))
             to_side(1, slot, 3, relay_sems, to_partner).start()
 
     def ready(step):
         for side in range(2):
             slot = slot_of(step, side)
-            to_side(2, slot, 2, partner_sems, here).wait_recv()
-            to_side(3, slot, 3, relay_sems, here).wait_recv()
+            got("wait_partner", to_side(2, slot, 2, partner_sems, here))
+            got("wait_relay", to_side(3, slot, 3, relay_sems, here))
 
     def far(slot):
         return send_of(far_out.at[slot], far_in.at[slot], far_sems, slot, to_across)
@@ -614,7 +660,7 @@
     def send_far(step):
         for side in range(2):
             slot = slot_of(step, side)
-            near(slot).wait_recv()
+            got("wait_near", near(slot))
             far_out[slot] = (part[slot, 1].astype(F32) + near_in[slot, 1].astype(F32)).astype(
                 BF16
             )
@@ -628,7 +674,7 @@
     def send_total(step):
         for side in range(2):
             slot = slot_of(step, side)
-            far(slot).wait_recv()
+            got("wait_far", far(slot))
             total[slot] = (
                 part[slot, 0].astype(F32)
                 + near_in[slot, 0].astype(F32)
@@ -637,34 +683,33 @@
             give_back(slot).start()
 
     def turn(step):
-        @pl.when((step >= 1) & (step < remote_lines))
+        relay(step - 1)
+        ready(step - 1)
+        timed("experts", experts, slot_of(step - 1, 0))
+        for side in range(2):
+            near(slot_of(step - 1, side)).start()
+
+        @pl.when(step + 1 < remote_lines)
         def next_line():
-            forward(step)
-            kv_step(step + 1)
-
-        @pl.when(step < remote_lines)
+            forward(step + 1)
+
+        send_far(step - 1)
+
+        @pl.when(step >= 2)
         def attend_line():
-            attend_step(step + 1)
-
-        @pl.when((step >= 1) & (step <= remote_lines))
-        def compute():
-            relay(step - 1)
-            ready(step - 1)
-            experts(slot_of(step - 1, 0))
-            for side in range(2):
-                near(slot_of(step - 1, side)).start()
+            attend_step(step - 1)
+
+        kv_step(step)
 
         @pl.when(step >= 2)
         def answer():
             send_total(step - 2)
 
-        @pl.when((step >= 1) & (step <= remote_lines))
-        def reduce_far():
-            send_far(step - 1)
-
     if remote_lines:
-        each(0, remote_lines + 2, turn)
-
+        each(1, remote_lines + 1, turn)
+
+    if remote_lines:
+        attend_step(remote_lines)
     weights[6].wait()
     rows_out = shard // tp_size
     mixer_term = jnp.dot(
@@ -679,37 +724,37 @@
     )
     mix_near_copy.start()
 
-    shared_near_copy.wait_recv()
-    pair_back.wait_recv()
+    got("wait_near_shared", shared_near_copy)
+    got("wait_pair_back", pair_back)
     far_shared_out[...] = (
         shared_acc[1] + near_shared[1].astype(F32) + mixed(pair_ep, 1, lambda: pair_in[1])
     ).astype(BF16)
     shared_far_copy = send_of(far_shared_out, far_shared, small_sems, FAR_SHARED, to_across)
     shared_far_copy.start()
-    mix_near_copy.wait_recv()
+    got("wait_near_mix", mix_near_copy)
     far_mix_out[...] = (mix_part[1].astype(F32) + near_mix[1].astype(F32)).astype(BF16)
     mix_far_copy = send_of(far_mix_out, far_mix, small_sems, FAR_MIX, to_across)
     mix_far_copy.start()
+    if remote_lines:
+        send_total(remote_lines - 1)
     result[...] = (
         shared_acc[0] + near_shared[0].astype(F32) + mixed(pair_ep, 0, lambda: pair_in[0])
     )
 
     def take_back(step):
         for side in range(2):
-            slot = slot_of(step, side)
+            slot = slot_to(step, side)
             block = back.at[slot]
-            send_of(block, block, return_sems, slot, here).wait_recv()
+            got("wait_back", send_of(block, block, return_sems, slot, here))
             result[...] = result[...] + mixed(to_ep(slot), 0, lambda: back[slot])
 
     each(0, remote_lines, take_back)
-    shared_far_copy.wait_recv()
-    combined = result[...] + far_shared[...].astype(F32)
-    expert_out[...] = root_norm(combined, exit_ref[...]).astype(BF16)
-    mix_far_copy.wait_recv()
-    mixer_sum = (
+    got("wait_far_shared", shared_far_copy)
+    expert_out[...] = result[...] + far_shared[...].astype(F32)
+    got("wait_far_mix", mix_far_copy)
+    mixer_out[...] = (
         mix_part[0].astype(F32) + near_mix[0].astype(F32) + far_mix[...].astype(F32)
     )
-    mixer_out[...] = root_norm(mixer_sum, mixer_gain_ref[...]).astype(BF16)
 
     own_copy(0, 1, 0, to_across).wait_send()
     own_copy(0, 2, 1, to_partner).wait_send()
@@ -755,6 +800,11 @@
     @pl.when(parity == 0)
     def sent_pair():
         kv_pair(kv_ref, 0).wait_send()
+
+
+def closing_norms(mixer_sum, expert_sum, mixer_gain, exit_gain, mixer_out, expert_out):
+    mixer_out[...] = root_norm(mixer_sum[...], mixer_gain[...]).astype(BF16)
+    expert_out[...] = root_norm(expert_sum[...], exit_gain[...]).astype(BF16)
 
 
 def on_device(
@@ -782,22 +832,16 @@
         ep_size, tp_size, key_bias.shape[1], query_rows, routed_input, expert_index, expert_gate
     )
     shard, width, model, rows = plan.shard, plan.width, plan.model, plan.rows
-    bias_rows = -(-plan.heads // 16) * 16
-    bias_block = jnp.pad(
-        jnp.transpose(key_bias), ((0, bias_rows - plan.heads), (0, 2 * width - shard))
-    )
-    kv_block = jnp.concatenate(
-        [jnp.concatenate([key_rows, value_rows], axis=1), bias_block], axis=0
-    )
+    kv_rows = shard + -(-plan.heads // 8) * 8
     small = [
         query_rows,
-        kv_block,
+        key_rows,
+        value_rows,
+        jnp.transpose(key_bias),
         routed_input,
         entry_gain.reshape(1, model),
-        exit_gain.reshape(1, model),
-        mixer_gain.reshape(1, model),
-        expert_index,
-        route_weights,
+        jnp.transpose(expert_index),
+        jnp.transpose(route_weights),
     ]
     large = [
         mixer_weight,
@@ -841,7 +885,8 @@
         buffer(2, *mix),
         buffer(*mix),
         buffer(*mix),
-        buffer(ep_size, *kv_block.shape),
+        buffer(kv_rows, 2 * width),
+        buffer(ep_size, kv_rows, 2 * width),
         buffer(plan.heads * shard, width),
         buffer(plan.heads * shard, shard, kind=F32),
         buffer(shard, width, kind=F32),
@@ -850,11 +895,11 @@
     scratch += [sem((len(large),))]
     for count in (4, 4, ep_size, ep_size, ep_size, ep_size, ep_size, ep_size, ep_size, ep_size, ep_size, 6):
         scratch += [sem((count,)), sem((count,))]
-    mixer_out, expert_out = pl.pallas_call(
+    mixer_sum, expert_sum = pl.pallas_call(
         functools.partial(layer_kernel, plan),
         out_shape=(
-            jax.ShapeDtypeStruct(mix, BF16),
-            jax.ShapeDtypeStruct((rows, model), BF16),
+            jax.ShapeDtypeStruct(mix, F32),
+            jax.ShapeDtypeStruct((rows, model), F32),
         ),
         in_specs=[vmem] * len(small) + [pl.BlockSpec(memory_space=pl.ANY)] * len(large),
         out_specs=(vmem, vmem),
@@ -864,7 +909,16 @@
         ),
         name="whole_layer",
     )(*small, *large)
-    return (mixer_out, expert_out)
+    return pl.pallas_call(
+        closing_norms,
+        out_shape=(
+            jax.ShapeDtypeStruct(mix, BF16),
+            jax.ShapeDtypeStruct((rows, model), BF16),
+        ),
+        in_specs=[vmem] * 4,
+        out_specs=(vmem, vmem),
+        name="closing_norms",
+    )(mixer_sum, expert_sum, mixer_gain.reshape(1, model), exit_gain.reshape(1, model))
 
 
 def solution(mesh):

time: 103 us -> 81.8 us (0.79)
  the two profiles are of different devices: /device:TPU:24 before, /device:TPU:0 now
where the time goes in v2:
time: 81.8 us; the launch traced here: 81.6 us
  Pallas kernels  81 us (99%)
    pallas_call x1, Pallas kernels, on_device(): pl.pallas_call(functools.partial(layer_kernel, plan), out_shape=(jax.Shap...  78.8 us
    pallas_call x1, Pallas kernels, on_device(): pl.pallas_call(closing_norms, out_shape=(jax.ShapeDtypeStruct(mix, BF16),...  2.19 us

profile of v2, /device:TPU:0, one launch (start us, length us, event | category | flops | bytes accessed | tf_op | source)
XLA Modules:
  0.0 81.6 jit_solution(5587431184227037816)
XLA Ops:
  0.6 78.8 %whole_layer.1 = (f32[32,2048]{1,0:T(8,128)}, f32[96,2048]{1,0:T(8,128)}) custom-call(bf16[128,256]{1,0:T(8,128)(2,1)} %refs_0_.1, bf16[128,256]{1,0:T(8,128)(2,1)} %refs_1_.1, bf16[128,256]{1,0:T(8,128)(2,1)} %refs_2_.1, bf16[4,128]{1,0:T(4,128)(2,1)} %bitcast.9, bf16[96,2048]{1,0:T(8,128)(2,1)} %refs_4_.1, f32[1,2048]{1,0:T(1,128)} %bitcast.8, ...), custom_call_target="tpu_custom_call" | custom-call | tf_op jit(solution)/shard_map/whole_layer/pallas_call | solution.py:898
  79.5 2.2 %closing_norms.1 = (bf16[32,2048]{1,0:T(8,128)(2,1)}, bf16[96,2048]{1,0:T(8,128)(2,1)}) custom-call(f32[32,2048]{1,0:T(8,128)} %get-tuple-element.4.mixer_sum, f32[96,2048]{1,0:T(8,128)} %get-tuple-element.5.expert_sum, f32[1,2048]{1,0:T(1,128)} %bitcast.6, f32[1,2048]{1,0:T(1,128)} %bitcast.7), custom_call_target="tpu_custom_call" | custom-call | tf_op jit(solution)/shard_map/closing_norms/pallas_call | solution.py:912

commit v3 on v2

--- a/solution.py
+++ b/solution.py
@@ -11,6 +11,7 @@
 EPS = 1e-06
 F32 = jnp.float32
 BF16 = jnp.bfloat16
+STRAIGHT = (0,)
 
 
 class Plan:
@@ -105,14 +106,16 @@
 
 def layer_kernel(plan, *refs):
     (
-        query_ref,
-        key_ref,
-        value_ref,
-        bias_ref,
-        input_ref,
-        entry_ref,
-        index_ref,
-        route_ref,
+        input_hbm,
+        entry_hbm,
+        index_hbm,
+        route_hbm,
+        key_hbm,
+        value_hbm,
+        bias_hbm,
+        query_hbm,
+        exit_hbm,
+        mixer_gain_hbm,
         mixer_hbm,
         gate_hbm,
         up_hbm,
@@ -122,6 +125,16 @@
         shared_down_hbm,
         mixer_out,
         expert_out,
+        input_ref,
+        entry_ref,
+        index_ref,
+        route_ref,
+        key_ref,
+        value_ref,
+        bias_ref,
+        query_ref,
+        exit_ref,
+        mixer_gain_ref,
         mixer_w,
         gate_w,
         up_w,
@@ -129,6 +142,7 @@
         shared_gate_w,
         shared_up_w,
         shared_down_w,
+        across_rows,
         own_all,
         info,
         info_cols,
@@ -143,6 +157,8 @@
         back,
         pair_out,
         pair_in,
+        twin_out,
+        twin_in,
         shared_acc,
         shared_near,
         near_shared,
@@ -158,6 +174,7 @@
         query_heads,
         carried,
         attended,
+        input_sem,
         weight_sem,
         own_send,
         own_recv,
@@ -213,7 +230,7 @@
     far_sems = (far_send, far_recv)
     return_sems = (return_send, return_recv)
     small_sems = (small_send, small_recv)
-    PAIR_ACROSS, PAIR_BACK, NEAR_SHARED, FAR_SHARED, NEAR_MIX, FAR_MIX = range(6)
+    PAIR_ACROSS, PAIR_BACK, NEAR_SHARED, FAR_SHARED, NEAR_MIX, FAR_MIX, TWIN = range(7)
 
     def to_ep(slot):
         return 2 * lax.rem(line + slot // 2, lines) + lax.rem(parity + slot, 2)
@@ -237,6 +254,10 @@
         near_line = jnp.where(upward, line + distance, line - distance)
         return jnp.where(step == 0, lax.rem(line + middle, lines), near_line)
 
+    twin = line + 1 - 2 * lax.rem(line, 2)
+    twin_from = 2 * lax.rem(line - twin + lines, lines)
+    twin_to = 2 * lax.rem(twin - line + lines, lines)
+
     def slot_of(step, side):
         return 2 * lax.rem(line - other_line(step) + lines, lines) + side
 
@@ -252,6 +273,26 @@
     each(1, ep_size, greet)
     for place in (partner_tp, across_tp, diagonal_tp):
         pl.semaphore_signal(barrier, inc=1, device_id=(own_ep, place), device_id_type=MESH)
+
+    inputs = [
+        pltpu.make_async_copy(source, target, input_sem.at[number])
+        for number, (source, target) in enumerate(
+            [
+                (input_hbm, input_ref),
+                (entry_hbm, entry_ref),
+                (index_hbm, index_ref),
+                (route_hbm, route_ref),
+                (key_hbm, key_ref),
+                (value_hbm, value_ref),
+                (bias_hbm, bias_ref),
+                (query_hbm, query_ref),
+                (exit_hbm, exit_ref),
+                (mixer_gain_hbm, mixer_gain_ref),
+            ]
+        )
+    ]
+    for copy in inputs:
+        copy.start()
 
     weights = [
         pltpu.make_async_copy(source, target, weight_sem.at[number])
@@ -270,16 +311,23 @@
     for copy in weights:
         copy.start()
 
-    normed = root_norm(input_ref[...].astype(F32), entry_ref[...]).astype(BF16)
-    own_all[0] = normed
-
+    inputs[0].wait()
     with jax.named_scope("wait_barrier"):
         pl.semaphore_wait(barrier, ep_size - 1 + 3)
 
     def own_copy(source, target, number, place):
         return send_of(own_all.at[source], own_all.at[target], own_sems, number, place)
 
-    own_copy(0, 1, 0, to_across).start()
+    rows_over_x = send_of(input_ref, across_rows, own_sems, 0, to_across)
+    rows_over_x.start()
+
+    def entry_norm(ref):
+        return root_norm(ref[...].astype(F32), entry_ref[...]).astype(BF16)
+
+    for copy in inputs[1:4]:
+        copy.wait()
+    normed = entry_norm(input_ref)
+    own_all[0] = normed
     own_copy(0, 2, 1, to_partner).start()
 
     expert_at = iota((plan.named, rows_n), 0)
@@ -328,6 +376,8 @@
 
         pack(chosen[slot * plan.picked : (slot + 1) * plan.picked], put_out)
 
+    for copy in inputs[4:]:
+        copy.wait()
     shard, width, heads = plan.shard, plan.width, plan.heads
     kv_ref[0:shard, 0:width] = key_ref[...]
     kv_ref[0:shard, width:] = value_ref[...]
@@ -455,7 +505,8 @@
     got("wait_pair", landed(1))
     to_side(0, 1, 2, partner_sems, to_partner).start()
 
-    got("wait_own_across", own_copy(1, 1, 0, here))
+    got("wait_own_across", rows_over_x)
+    own_all[1] = entry_norm(across_rows)
     own_copy(1, 3, 2, to_partner).start()
     info_copy(1, 1, here).wait_recv()
 
@@ -485,6 +536,11 @@
 
     if remote_lines:
         forward_side(0, 0)
+
+    def relay(step, side):
+        slot = slot_of(step, side)
+        got("wait_across", to_side(1, slot, 1, across_sems, here))
+        to_side(1, slot, 3, relay_sems, to_partner).start()
 
     got("wait_own_partner", own_copy(2, 2, 1, here))
     got("wait_own_diag", own_copy(3, 3, 2, here))
@@ -628,6 +684,8 @@
             shared_acc[rel] = shared_acc[rel] + mixed(own_ep, rel, lambda rel=rel: part[0, rel])
 
     timed("fold_own", fold_own)
+    if remote_lines:
+        relay(0, 0)
     shared_near[...] = shared_acc[2:4].astype(BF16)
     shared_near_copy = send_of(shared_near, near_shared, small_sems, NEAR_SHARED, to_partner)
     shared_near_copy.start()
@@ -642,11 +700,9 @@
         got("wait_kv_pair", send_of(block, block, kv_pair_sems, 0, here))
         timed("attend", attend_slot, 1)
 
-    def relay(step):
-        for side in range(2):
-            slot = slot_of(step, side)
-            got("wait_across", to_side(1, slot, 1, across_sems, here))
-            to_side(1, slot, 3, relay_sems, to_partner).start()
+    if remote_lines:
+        kv_step(1)
+
 
     def ready(step):
         for side in range(2):
@@ -657,14 +713,36 @@
     def far(slot):
         return send_of(far_out.at[slot], far_in.at[slot], far_sems, slot, to_across)
 
+    def twin_copy(side):
+        return send_of(
+            twin_out.at[side],
+            twin_in.at[side],
+            small_sems,
+            TWIN + side,
+            (from_ep(twin_from + side), own_tp),
+        )
+
     def send_far(step):
+        is_twin = other_line(step) == twin
         for side in range(2):
             slot = slot_of(step, side)
             got("wait_near", near(slot))
-            far_out[slot] = (part[slot, 1].astype(F32) + near_in[slot, 1].astype(F32)).astype(
-                BF16
-            )
-            far(slot).start()
+
+            def over_x(slot=slot):
+                value = part[slot, 1].astype(F32) + near_in[slot, 1].astype(F32)
+                far_out[slot] = value.astype(BF16)
+                far(slot).start()
+
+            def straight(slot=slot, side=side):
+                value = part[slot, 0:2].astype(F32) + near_in[slot].astype(F32)
+                twin_out[side] = value.astype(BF16)
+                twin_copy(side).start()
+
+            if side in STRAIGHT:
+                pl.when(is_twin)(straight)
+                pl.when(jnp.logical_not(is_twin))(over_x)
+            else:
+                over_x()
 
     def give_back(slot):
         return send_of(
@@ -672,8 +750,7 @@
         )
 
     def send_total(step):
-        for side in range(2):
-            slot = slot_of(step, side)
+        def reduced(slot):
             got("wait_far", far(slot))
             total[slot] = (
                 part[slot, 0].astype(F32)
@@ -682,24 +759,37 @@
             ).astype(BF16)
             give_back(slot).start()
 
+        for side in range(2):
+            if side in STRAIGHT:
+                pl.when(other_line(step) != twin)(
+                    functools.partial(reduced, slot_of(step, side))
+                )
+            else:
+                reduced(slot_of(step, side))
+
     def turn(step):
-        relay(step - 1)
+        @pl.when(step >= 2)
+        def relay_first():
+            relay(step - 1, 0)
+
+        relay(step - 1, 1)
+
+        @pl.when(step >= 3)
+        def attend_line():
+            attend_step(step - 2)
+
         ready(step - 1)
         timed("experts", experts, slot_of(step - 1, 0))
         for side in range(2):
             near(slot_of(step - 1, side)).start()
 
+        send_far(step - 1)
+
         @pl.when(step + 1 < remote_lines)
         def next_line():
             forward(step + 1)
 
-        send_far(step - 1)
-
-        @pl.when(step >= 2)
-        def attend_line():
-            attend_step(step - 1)
-
-        kv_step(step)
+        kv_step(step + 1)
 
         @pl.when(step >= 2)
         def answer():
@@ -708,8 +798,25 @@
     if remote_lines:
         each(1, remote_lines + 1, turn)
 
+    def folded_rows(rel):
+        value = shared_acc[rel] + near_shared[rel].astype(F32)
+        value = value + mixed(pair_ep, rel, lambda: pair_in[rel])
+        if remote_lines:
+            for side in STRAIGHT:
+                value = value + mixed(
+                    to_ep(twin_to + side), rel, lambda side=side: twin_in[side, rel]
+                )
+        return value
+
+    got("wait_near_shared", shared_near_copy)
+    got("wait_pair_back", pair_back)
     if remote_lines:
-        attend_step(remote_lines)
+        for side in STRAIGHT:
+            got("wait_twin", twin_copy(side))
+    far_shared_out[...] = folded_rows(1).astype(BF16)
+    shared_far_copy = send_of(far_shared_out, far_shared, small_sems, FAR_SHARED, to_across)
+    shared_far_copy.start()
+    each(max(remote_lines - 1, 1), remote_lines + 1, attend_step)
     weights[6].wait()
     rows_out = shard // tp_size
     mixer_term = jnp.dot(
@@ -723,40 +830,15 @@
         mix_part.at[pl.ds(2, 2)], near_mix, small_sems, NEAR_MIX, to_partner
     )
     mix_near_copy.start()
-
-    got("wait_near_shared", shared_near_copy)
-    got("wait_pair_back", pair_back)
-    far_shared_out[...] = (
-        shared_acc[1] + near_shared[1].astype(F32) + mixed(pair_ep, 1, lambda: pair_in[1])
-    ).astype(BF16)
-    shared_far_copy = send_of(far_shared_out, far_shared, small_sems, FAR_SHARED, to_across)
-    shared_far_copy.start()
+    if remote_lines:
+        send_total(remote_lines - 1)
     got("wait_near_mix", mix_near_copy)
     far_mix_out[...] = (mix_part[1].astype(F32) + near_mix[1].astype(F32)).astype(BF16)
     mix_far_copy = send_of(far_mix_out, far_mix, small_sems, FAR_MIX, to_across)
     mix_far_copy.start()
-    if remote_lines:
-        send_total(remote_lines - 1)
-    result[...] = (
-        shared_acc[0] + near_shared[0].astype(F32) + mixed(pair_ep, 0, lambda: pair_in[0])
-    )
-
-    def take_back(step):
-        for side in range(2):
-            slot = slot_to(step, side)
-            block = back.at[slot]
-            got("wait_back", send_of(block, block, return_sems, slot, here))
-            result[...] = result[...] + mixed(to_ep(slot), 0, lambda: back[slot])
-
-    each(0, remote_lines, take_back)
-    got("wait_far_shared", shared_far_copy)
-    expert_out[...] = result[...] + far_shared[...].astype(F32)
-    got("wait_far_mix", mix_far_copy)
-    mixer_out[...] = (
-        mix_part[0].astype(F32) + near_mix[0].astype(F32) + far_mix[...].astype(F32)
-    )
-
-    own_copy(0, 1, 0, to_across).wait_send()
+    result[...] = folded_rows(0)
+
+    rows_over_x.wait_send()
     own_copy(0, 2, 1, to_partner).wait_send()
     own_copy(1, 3, 2, to_partner).wait_send()
     for target, place in ((1, to_across), (2, to_partner), (3, to_diagonal)):
@@ -765,15 +847,14 @@
     to_side(0, 1, 2, partner_sems, to_partner).wait_send()
     to_side(1, 1, 3, relay_sems, to_partner).wait_send()
     near(1).wait_send()
-    for copy in (
-        pair_across,
-        pair_back,
-        shared_near_copy,
-        shared_far_copy,
-        mix_near_copy,
-        mix_far_copy,
-    ):
+    for copy in (pair_across, pair_back, shared_near_copy, mix_near_copy):
         copy.wait_send()
+
+    def is_straight(slot):
+        found = slot < 0
+        for side in STRAIGHT:
+            found = found | (slot == twin_from + side)
+        return found
 
     def finish(slot):
         go(slot).wait_send()
@@ -781,10 +862,16 @@
         to_side(0, slot, 2, partner_sems, to_partner).wait_send()
         to_side(1, slot, 3, relay_sems, to_partner).wait_send()
         near(slot).wait_send()
-        far(slot).wait_send()
-        give_back(slot).wait_send()
+
+        @pl.when(jnp.logical_not(is_straight(slot)))
+        def reduced():
+            far(slot).wait_send()
 
     each(2, ep_size, finish)
+
+    if remote_lines:
+        for side in STRAIGHT:
+            twin_copy(side).wait_send()
 
     def finish_kv(step):
         @pl.when((step <= line) & (line + 1 < lines))
@@ -801,10 +888,39 @@
     def sent_pair():
         kv_pair(kv_ref, 0).wait_send()
 
-
-def closing_norms(mixer_sum, expert_sum, mixer_gain, exit_gain, mixer_out, expert_out):
-    mixer_out[...] = root_norm(mixer_sum[...], mixer_gain[...]).astype(BF16)
-    expert_out[...] = root_norm(expert_sum[...], exit_gain[...]).astype(BF16)
+    def take_back(step):
+        def one(slot):
+            block = back.at[slot]
+            got("wait_back", send_of(block, block, return_sems, slot, here))
+            result[...] = result[...] + mixed(to_ep(slot), 0, lambda: back[slot])
+
+        for side in range(2):
+            if side in STRAIGHT:
+                pl.when(other_line(step) != twin)(functools.partial(one, slot_to(step, side)))
+            else:
+                one(slot_to(step, side))
+
+    each(0, remote_lines, take_back)
+
+    def returned(slot):
+        @pl.when(jnp.logical_not(is_straight(slot)))
+        def one():
+            give_back(slot).wait_send()
+
+    each(2, ep_size, returned)
+    got("wait_far_shared", shared_far_copy)
+    combined = result[...] + far_shared[...].astype(F32)
+    expert_out[...] = root_norm(combined, exit_ref[...]).astype(BF16)
+    got("wait_far_mix", mix_far_copy)
+    mixer_sum = mix_part[0].astype(F32) + near_mix[0].astype(F32) + far_mix[...].astype(F32)
+    mixer_out[...] = root_norm(mixer_sum, mixer_gain_ref[...]).astype(BF16)
+    shared_far_copy.wait_send()
+    mix_far_copy.wait_send()
+
+
+def hand_on(mixer_in, expert_in, mixer_out, expert_out):
+    mixer_out[...] = mixer_in[...]
+    expert_out[...] = expert_in[...]
 
 
 def on_device(
@@ -834,14 +950,16 @@
     shard, width, model, rows = plan.shard, plan.width, plan.model, plan.rows
     kv_rows = shard + -(-plan.heads // 8) * 8
     small = [
-        query_rows,
-        key_rows,
-        value_rows,
-        jnp.transpose(key_bias),
         routed_input,
         entry_gain.reshape(1, model),
         jnp.transpose(expert_index),
         jnp.transpose(route_weights),
+        key_rows,
+        value_rows,
+        jnp.transpose(key_bias),
+        query_rows,
+        exit_gain.reshape(1, model),
+        mixer_gain.reshape(1, model),
     ]
     large = [
         mixer_weight,
@@ -859,8 +977,9 @@
     def buffer(*shape, kind=BF16):
         return pltpu.VMEM(shape, kind)
 
-    scratch = [pltpu.VMEM(value.shape, value.dtype) for value in large]
+    scratch = [pltpu.VMEM(value.shape, value.dtype) for value in small + large]
     scratch += [
+        buffer(rows, model),
         buffer(tp_size, rows, model),
         buffer(tp_size, 8, plan.padded_rows, kind=F32),
         buffer(tp_size, plan.padded_rows, 128, kind=F32),
@@ -875,6 +994,8 @@
         buffer(ep_size, *block),
         buffer(2, *block),
         buffer(2, *block),
+        buffer(2, 2, *block),
+        buffer(2, 2, *block),
         buffer(tp_size, rows, model, kind=F32),
         buffer(2, rows, model),
         buffer(2, rows, model),
@@ -892,16 +1013,16 @@
         buffer(shard, width, kind=F32),
     ]
     sem = pltpu.SemaphoreType.DMA
-    scratch += [sem((len(large),))]
-    for count in (4, 4, ep_size, ep_size, ep_size, ep_size, ep_size, ep_size, ep_size, ep_size, ep_size, 6):
+    scratch += [sem((len(small),)), sem((len(large),))]
+    for count in (4, 4, ep_size, ep_size, ep_size, ep_size, ep_size, ep_size, ep_size, ep_size, ep_size, 8):
         scratch += [sem((count,)), sem((count,))]
-    mixer_sum, expert_sum = pl.pallas_call(
+    results = pl.pallas_call(
         functools.partial(layer_kernel, plan),
         out_shape=(
-            jax.ShapeDtypeStruct(mix, F32),
-            jax.ShapeDtypeStruct((rows, model), F32),
+            jax.ShapeDtypeStruct(mix, BF16),
+            jax.ShapeDtypeStruct((rows, model), BF16),
         ),
-        in_specs=[vmem] * len(small) + [pl.BlockSpec(memory_space=pl.ANY)] * len(large),
+        in_specs=[pl.BlockSpec(memory_space=pltpu.HBM)] * len(small + large),
         out_specs=(vmem, vmem),
         scratch_shapes=scratch,
         compiler_params=pltpu.CompilerParams(
@@ -910,15 +1031,15 @@
         name="whole_layer",
     )(*small, *large)
     return pl.pallas_call(
-        closing_norms,
+        hand_on,
         out_shape=(
             jax.ShapeDtypeStruct(mix, BF16),
             jax.ShapeDtypeStruct((rows, model), BF16),
         ),
-        in_specs=[vmem] * 4,
+        in_specs=[vmem] * 2,
         out_specs=(vmem, vmem),
-        name="closing_norms",
-    )(mixer_sum, expert_sum, mixer_gain.reshape(1, model), exit_gain.reshape(1, model))
+        name="hand_on",
+    )(*results)
 
 
 def solution(mesh):

time: 81.8 us -> 77.4 us (0.946); the launches traced: 81.6 us -> 76.4 us
  Pallas kernels: 81 us -> 75.8 us
    pallas_call x1, Pallas kernels: 78.8 us -> 73.9 us  [on_device(): pl.pallas_call(functools.partial(layer_kernel, plan), out_shape=(jax.Shap...]
where the time goes in v3:
time: 77.4 us; the launch traced here: 76.4 us
  Pallas kernels  75.8 us (98%)
    pallas_call x1, Pallas kernels, on_device(): pl.pallas_call(functools.partial(layer_kernel, plan), out_shape=(jax.Shap...  73.9 us
    pallas_call x1, Pallas kernels, on_device(): pl.pallas_call(hand_on, out_shape=(jax.ShapeDtypeStruct(mix, BF16), jax.S...  1.87 us

profile of v3, /device:TPU:0, one launch (start us, length us, event | category | flops | bytes accessed | tf_op | source)
XLA Modules:
  0.0 76.4 jit_solution(13656234838661133767)
XLA Ops:
  0.6 73.9 %whole_layer.1 = (bf16[32,2048]{1,0:T(8,128)(2,1)}, bf16[96,2048]{1,0:T(8,128)(2,1)}) custom-call(bf16[96,2048]{1,0:T(8,128)(2,1)} %refs_0_.1, f32[1,2048]{1,0:T(1,128)} %bitcast.6, s32[2,96]{1,0:T(2,128)} %bitcast.9, f32[2,96]{1,0:T(2,128)} %bitcast.10, bf16[128,256]{1,0:T(8,128)(2,1)} %refs_4_.1, bf16[128,256]{1,0:T(8,128)(2,1)} %refs_5_.1, ...), custom_call_target="tpu_custom_call" | custom-call | tf_op jit(solution)/shard_map/whole_layer/pallas_call | solution.py:1019
  74.5 1.9 %hand_on.1 = (bf16[32,2048]{1,0:T(8,128)(2,1)}, bf16[96,2048]{1,0:T(8,128)(2,1)}) custom-call(bf16[32,2048]{1,0:T(8,128)(2,1)} %get-tuple-element.4.mixer_in, bf16[96,2048]{1,0:T(8,128)(2,1)} %get-tuple-element.5.expert_in), custom_call_target="tpu_custom_call" | custom-call | tf_op jit(solution)/shard_map/hand_on/pallas_call | solution.py:1033

commit v4 on v3

--- a/solution.py
+++ b/solution.py
@@ -123,8 +123,11 @@
         shared_gate_hbm,
         shared_up_hbm,
         shared_down_hbm,
+        mixer_hbm_out,
+        expert_hbm_out,
         mixer_out,
         expert_out,
+        output_sem,
         input_ref,
         entry_ref,
         index_ref,
@@ -245,10 +248,10 @@
 
     def other_line(step):
         middle = lines // 2
-        inner = jnp.minimum(line, lines - 1 - line)
-        index = jnp.where(step <= middle + inner - 1, step - 1, step)
-        around = index < 2 * inner
-        distance = jnp.where(around, index // 2 + 1, index - inner + 1)
+        margin = jnp.minimum(line, lines - 1 - line)
+        index = jnp.where(step <= middle + margin - 1, step - 1, step)
+        around = index < 2 * margin
+        distance = jnp.where(around, index // 2 + 1, index - margin + 1)
         to_end = jnp.where(around, lax.rem(index, 2), 1)
         upward = (2 * line < lines) == (to_end == 1)
         near_line = jnp.where(upward, line + distance, line - distance)
@@ -257,6 +260,8 @@
     twin = line + 1 - 2 * lax.rem(line, 2)
     twin_from = 2 * lax.rem(line - twin + lines, lines)
     twin_to = 2 * lax.rem(twin - line + lines, lines)
+    outer = (lax.rem(line, 2) == 0) == (2 * line < lines)
+    inner = jnp.logical_not(outer)
 
     def slot_of(step, side):
         return 2 * lax.rem(line - other_line(step) + lines, lines) + side
@@ -723,7 +728,7 @@
         )
 
     def send_far(step):
-        is_twin = other_line(step) == twin
+        is_twin = (other_line(step) == twin) & outer
         for side in range(2):
             slot = slot_of(step, side)
             got("wait_near", near(slot))
@@ -761,7 +766,7 @@
 
         for side in range(2):
             if side in STRAIGHT:
-                pl.when(other_line(step) != twin)(
+                pl.when((other_line(step) != twin) | inner)(
                     functools.partial(reduced, slot_of(step, side))
                 )
             else:
@@ -800,20 +805,28 @@
 
     def folded_rows(rel):
         value = shared_acc[rel] + near_shared[rel].astype(F32)
-        value = value + mixed(pair_ep, rel, lambda: pair_in[rel])
-        if remote_lines:
-            for side in STRAIGHT:
-                value = value + mixed(
-                    to_ep(twin_to + side), rel, lambda side=side: twin_in[side, rel]
-                )
-        return value
+        return value + mixed(pair_ep, rel, lambda: pair_in[rel])
+
+    def fold_twin(rel):
+        value = result[...]
+        for side in STRAIGHT:
+            value = value + mixed(
+                to_ep(twin_to + side), rel, lambda side=side: twin_in[side, rel]
+            )
+        result[...] = value
 
     got("wait_near_shared", shared_near_copy)
     got("wait_pair_back", pair_back)
+    result[...] = folded_rows(1)
     if remote_lines:
-        for side in STRAIGHT:
-            got("wait_twin", twin_copy(side))
-    far_shared_out[...] = folded_rows(1).astype(BF16)
+
+        @pl.when(inner)
+        def with_twin():
+            for side in STRAIGHT:
+                got("wait_twin", twin_copy(side))
+            fold_twin(1)
+
+    far_shared_out[...] = result[...].astype(BF16)
     shared_far_copy = send_of(far_shared_out, far_shared, small_sems, FAR_SHARED, to_across)
     shared_far_copy.start()
     each(max(remote_lines - 1, 1), remote_lines + 1, attend_step)
@@ -837,6 +850,8 @@
     mix_far_copy = send_of(far_mix_out, far_mix, small_sems, FAR_MIX, to_across)
     mix_far_copy.start()
     result[...] = folded_rows(0)
+    if remote_lines:
+        pl.when(inner)(functools.partial(fold_twin, 0))
 
     rows_over_x.wait_send()
     own_copy(0, 2, 1, to_partner).wait_send()
@@ -853,7 +868,7 @@
     def is_straight(slot):
         found = slot < 0
         for side in STRAIGHT:
-            found = found | (slot == twin_from + side)
+            found = found | ((slot == twin_from + side) & outer)
         return found
 
     def finish(slot):
@@ -870,8 +885,11 @@
     each(2, ep_size, finish)
 
     if remote_lines:
-        for side in STRAIGHT:
-            twin_copy(side).wait_send()
+
+        @pl.when(outer)
+        def sent_twin():
+            for side in STRAIGHT:
+                twin_copy(side).wait_send()
 
     def finish_kv(step):
         @pl.when((step <= line) & (line + 1 < lines))
@@ -896,7 +914,9 @@
 
         for side in range(2):
             if side in STRAIGHT:
-                pl.when(other_line(step) != twin)(functools.partial(one, slot_to(step, side)))
+                pl.when((other_line(step) != twin) | outer)(
+                    functools.partial(one, slot_to(step, side))
+                )
             else:
                 one(slot_to(step, side))
 
@@ -907,20 +927,43 @@
         def one():
             give_back(slot).wait_send()
 
-    each(2, ep_size, returned)
+    timed("drain_returns", each, 2, ep_size, returned)
     got("wait_far_shared", shared_far_copy)
-    combined = result[...] + far_shared[...].astype(F32)
-    expert_out[...] = root_norm(combined, exit_ref[...]).astype(BF16)
+    with jax.named_scope("final_expert"):
+        combined = result[...] + far_shared[...].astype(F32)
+        expert_out[...] = root_norm(combined, exit_ref[...]).astype(BF16)
+    expert_write = pltpu.make_async_copy(expert_out, expert_hbm_out, output_sem.at[0])
+    expert_write.start()
     got("wait_far_mix", mix_far_copy)
-    mixer_sum = mix_part[0].astype(F32) + near_mix[0].astype(F32) + far_mix[...].astype(F32)
-    mixer_out[...] = root_norm(mixer_sum, mixer_gain_ref[...]).astype(BF16)
+    with jax.named_scope("final_mixer"):
+        mixer_sum = mix_part[0].astype(F32) + near_mix[0].astype(F32) + far_mix[...].astype(F32)
+        mixer_out[...] = root_norm(mixer_sum, mixer_gain_ref[...]).astype(BF16)
+    mixer_write = pltpu.make_async_copy(mixer_out, mixer_hbm_out, output_sem.at[1])
+    mixer_write.start()
     shared_far_copy.wait_send()
     mix_far_copy.wait_send()
-
-
-def hand_on(mixer_in, expert_in, mixer_out, expert_out):
-    mixer_out[...] = mixer_in[...]
-    expert_out[...] = expert_in[...]
+    with jax.named_scope("writes"):
+        expert_write.wait()
+        mixer_write.wait()
+
+
+def hand_on(mixer_in, expert_in, mixer_out, expert_out, mixer_held, expert_held, sems):
+    arrays = [(expert_in, expert_held, expert_out), (mixer_in, mixer_held, mixer_out)]
+    reads = [
+        pltpu.make_async_copy(source, held, sems.at[0, number])
+        for number, (source, held, target) in enumerate(arrays)
+    ]
+    writes = [
+        pltpu.make_async_copy(held, target, sems.at[1, number])
+        for number, (source, held, target) in enumerate(arrays)
+    ]
+    for read in reads:
+        read.start()
+    for read, write in zip(reads, writes):
+        read.wait()
+        write.start()
+    for write in writes:
+        write.wait()
 
 
 def on_device(
@@ -970,14 +1013,16 @@
         shared_up,
         shared_down,
     ]
-    vmem = pl.BlockSpec(memory_space=pltpu.VMEM)
     block = (plan.block, plan.half)
     mix = (shard // tp_size, model)
 
     def buffer(*shape, kind=BF16):
         return pltpu.VMEM(shape, kind)
 
-    scratch = [pltpu.VMEM(value.shape, value.dtype) for value in small + large]
+    sem = pltpu.SemaphoreType.DMA
+    hbm = pl.BlockSpec(memory_space=pltpu.HBM)
+    scratch = [buffer(*mix), buffer(rows, model), sem((2,))]
+    scratch += [pltpu.VMEM(value.shape, value.dtype) for value in small + large]
     scratch += [
         buffer(rows, model),
         buffer(tp_size, rows, model),
@@ -1012,7 +1057,6 @@
         buffer(plan.heads * shard, shard, kind=F32),
         buffer(shard, width, kind=F32),
     ]
-    sem = pltpu.SemaphoreType.DMA
     scratch += [sem((len(small),)), sem((len(large),))]
     for count in (4, 4, ep_size, ep_size, ep_size, ep_size, ep_size, ep_size, ep_size, ep_size, ep_size, 8):
         scratch += [sem((count,)), sem((count,))]
@@ -1022,8 +1066,8 @@
             jax.ShapeDtypeStruct(mix, BF16),
             jax.ShapeDtypeStruct((rows, model), BF16),
         ),
-        in_specs=[pl.BlockSpec(memory_space=pltpu.HBM)] * len(small + large),
-        out_specs=(vmem, vmem),
+        in_specs=[hbm] * len(small + large),
+        out_specs=(hbm, hbm),
         scratch_shapes=scratch,
         compiler_params=pltpu.CompilerParams(
             collective_id=0, has_side_effects=True, vmem_limit_bytes=62 * 1024 * 1024
@@ -1036,8 +1080,9 @@
             jax.ShapeDtypeStruct(mix, BF16),
             jax.ShapeDtypeStruct((rows, model), BF16),
         ),
-        in_specs=[vmem] * 2,
-        out_specs=(vmem, vmem),
+        in_specs=[hbm] * 2,
+        out_specs=(hbm, hbm),
+        scratch_shapes=[buffer(*mix), buffer(rows, model), sem((2, 2))],
         name="hand_on",
     )(*results)
 

time: 77.4 us -> 76.6 us (0.990)
  no operation moved by 1% of the time
where the time goes in v4:
time: 76.6 us; the launch traced here: 76.2 us
  Pallas kernels  75.5 us (99%)
    pallas_call x1, Pallas kernels, on_device(): pl.pallas_call(functools.partial(layer_kernel, plan), out_shape=(jax.Shap...  73.7 us
    pallas_call x1, Pallas kernels, on_device(): pl.pallas_call(hand_on, out_shape=(jax.ShapeDtypeStruct(mix, BF16), jax.S...  1.81 us

profile of v4, /device:TPU:0, one launch (start us, length us, event | category | flops | bytes accessed | tf_op | source)
XLA Modules:
  0.0 76.2 jit_solution(6109366284344224583)
XLA Ops:
  0.6 73.7 %whole_layer.1 = (bf16[32,2048]{1,0:T(8,128)(2,1)}, bf16[96,2048]{1,0:T(8,128)(2,1)}) custom-call(bf16[96,2048]{1,0:T(8,128)(2,1)} %refs_0_.1, f32[1,2048]{1,0:T(1,128)} %bitcast.6, s32[2,96]{1,0:T(2,128)} %bitcast.9, f32[2,96]{1,0:T(2,128)} %bitcast.10, bf16[128,256]{1,0:T(8,128)(2,1)} %refs_4_.1, bf16[128,256]{1,0:T(8,128)(2,1)} %refs_5_.1, ...), custom_call_target="tpu_custom_call" | custom-call | tf_op jit(solution)/shard_map/whole_layer/pallas_call | solution.py:1063
  74.4 1.8 %hand_on.1 = (bf16[32,2048]{1,0:T(8,128)(2,1)}, bf16[96,2048]{1,0:T(8,128)(2,1)}) custom-call(bf16[32,2048]{1,0:T(8,128)(2,1)} %get-tuple-element.4.mixer_in, bf16[96,2048]{1,0:T(8,128)(2,1)} %get-tuple-element.5.expert_in), custom_call_target="tpu_custom_call" | custom-call | tf_op jit(solution)/shard_map/hand_on/pallas_call | solution.py:1077

commit v5 on v4

--- a/solution.py
+++ b/solution.py
@@ -794,11 +794,11 @@
         def next_line():
             forward(step + 1)
 
-        kv_step(step + 1)
-
         @pl.when(step >= 2)
         def answer():
             send_total(step - 2)
+
+        kv_step(step + 1)
 
     if remote_lines:
         each(1, remote_lines + 1, turn)

time: 76.6 us -> 78.5 us (1.025)
  Pallas kernels: 75.5 us -> 77.7 us
    pallas_call x1, Pallas kernels: 73.7 us -> 75.9 us  [on_device(): pl.pallas_call(functools.partial(layer_kernel, plan), out_shape=(jax.Shap...]
where the time goes in v5:
time: 78.5 us; the launch traced here: 78.4 us
  Pallas kernels  77.7 us (99%)
    pallas_call x1, Pallas kernels, on_device(): pl.pallas_call(functools.partial(layer_kernel, plan), out_shape=(jax.Shap...  75.9 us
    pallas_call x1, Pallas kernels, on_device(): pl.pallas_call(hand_on, out_shape=(jax.ShapeDtypeStruct(mix, BF16), jax.S...  1.81 us

profile of v5, /device:TPU:0, one launch (start us, length us, event | category | flops | bytes accessed | tf_op | source)
XLA Modules:
  0.0 78.4 jit_solution(3318043188009088434)
XLA Ops:
  0.6 75.9 %whole_layer.1 = (bf16[32,2048]{1,0:T(8,128)(2,1)}, bf16[96,2048]{1,0:T(8,128)(2,1)}) custom-call(bf16[96,2048]{1,0:T(8,128)(2,1)} %refs_0_.1, f32[1,2048]{1,0:T(1,128)} %bitcast.6, s32[2,96]{1,0:T(2,128)} %bitcast.9, f32[2,96]{1,0:T(2,128)} %bitcast.10, bf16[128,256]{1,0:T(8,128)(2,1)} %refs_4_.1, bf16[128,256]{1,0:T(8,128)(2,1)} %refs_5_.1, ...), custom_call_target="tpu_custom_call" | custom-call | tf_op jit(solution)/shard_map/whole_layer/pallas_call | solution.py:1063
  76.5 1.8 %hand_on.1 = (bf16[32,2048]{1,0:T(8,128)(2,1)}, bf16[96,2048]{1,0:T(8,128)(2,1)}) custom-call(bf16[32,2048]{1,0:T(8,128)(2,1)} %get-tuple-element.4.mixer_in, bf16[96,2048]{1,0:T(8,128)(2,1)} %get-tuple-element.5.expert_in), custom_call_target="tpu_custom_call" | custom-call | tf_op jit(solution)/shard_map/hand_on/pallas_call | solution.py:1077
